TPU v7x, 512 devices: a whole 4x4x16 slice. The times are simulated.
512 devices in a mesh: ep: 32 (over z, core), tp: 16 (over y, x).
Axes of the slice: x: 4, y: 4, z: 16, core: 2. Of those that a mesh axis runs over, the one named last changes fastest.
Arguments:
- first_batch_queries: bfloat16 [8192, 1024], P('ep', 'tp'), may hold values from -6 to 6
- first_batch_keys: bfloat16 [8192, 1024], P('ep', 'tp'), may hold values from -6 to 6
- first_batch_values: bfloat16 [8192, 2048], P('ep', 'tp'), may hold values from -6 to 6
- output_gate_preactivation: bfloat16 [8192, 2048], P('ep', 'tp'), may hold values from -6 to 6
- decay_preactivation: bfloat16 [8192, 1024], P('ep', 'tp'), may hold values from -6 to 6
- channel_decay_bias: float32 [1024], P('tp')
- added_log_decay: float32 [16, 8192], P('tp', 'ep'), may hold values from -0.7 to 0
- head_norm_gain: float32 [2048], P('tp'), may hold values from 0.1 to 1.9
- attention_output_weight: bfloat16 [2048, 2048], P(None, 'tp'), may hold values from -0.125 to 0.125
- second_batch_rows: bfloat16 [3072, 2048], P('ep'), may hold values from -6 to 6
- expert_norm_gain: float32 [2048], replicated, may hold values from 0.1 to 1.9
- routed_expert_index: int32 [3072, 4], P('ep'), may hold values from 0 to 31, all different within a row; in each aligned block of 96 rows (0 to 95, 96 to 191, ...) at most 18 rows name the same one
- router_chosen_scores: float32 [3072, 4], P('ep'), may hold values from 0.1 to 1
- expert_gate_weight: bfloat16 [32, 2048, 4096], P('ep', None, 'tp'), may hold values from -0.125 to 0.125
- expert_up_weight: bfloat16 [32, 2048, 4096], P('ep', None, 'tp'), may hold values from -0.125 to 0.125
- expert_down_weight: bfloat16 [32, 4096, 2048], P('ep', None, 'tp'), may hold values from -0.09375 to 0.09375
- shared_gate_weight: bfloat16 [2048, 1024], P(None, 'tp'), may hold values from -0.125 to 0.125
- shared_up_weight: bfloat16 [2048, 1024], P(None, 'tp'), may hold values from -0.125 to 0.125
- shared_down_weight: bfloat16 [1024, 2048], P(None, 'tp'), may hold values from -0.1875 to 0.1875
Outputs:
- token_mixed: bfloat16 [8192, 2048], P('ep', 'tp')
- channel_mixed: bfloat16 [3072, 2048], P('ep', 'tp')
Inputs may be any that keep to these rules, and one draw needn't show every extreme that they name: `routed_expert_index`: in each aligned block of 96 rows (the rows of one index of ep) no expert is named by more than 18 rows, a bound that some block reaches; a row names 4 different experts.
All inputs are finite; a program needn't handle non-finite values.
Results may differ from a plain program's by a relative error of at most 0.018.
Values may be sent and summed in bfloat16 or wider, within the bound.
A program may use at most 64 MiB of HBM per device.

v0:
```python
import jax
import jax.numpy as jnp
from jax import lax
from jax.sharding import Mesh
from jax.sharding import PartitionSpec as P

BLOCK = 64
EP = ("ep_0", "ep_1")


epsilon = 1e-06
temper = 16.0
routed_scale = 2.5


def nothing_yet(value, identity):
    return jax.tree.map(
        lambda a, e: jnp.broadcast_to(jnp.asarray(e, a.dtype), a.shape), value, identity
    )


def collected_together(value, axis):
    leaves = jax.tree.leaves(value)
    order = sorted(range(len(leaves)), key=lambda k: -leaves[k].size)
    width = (1, *leaves[order[0]].shape)[-1]
    lines = [
        jnp.pad(leaves[k].reshape(-1), (0, -leaves[k].size % width)).reshape(-1, width)
        for k in order
    ]
    both, at, found = (lax.all_gather(jnp.concatenate(lines), axis), 0, {})
    for k, line in zip(order, lines):
        piece = both[:, at : at + len(line)].reshape(len(both), -1)
        found[k] = piece[:, : leaves[k].size].reshape(-1, *leaves[k].shape)
        at += len(line)
    numbers = iter(range(len(leaves)))
    return jax.tree.map(lambda _: found[next(numbers)], value)


def carried_in(value, axes, combine, identity):
    before = start = nothing_yet(value, identity)
    total = value
    for axis in reversed(axes):
        size, here = (lax.axis_size(axis), lax.axis_index(axis))
        pieces = collected_together(
            jax.tree.map(lambda part, kind: part.astype(kind), total, (jnp.bfloat16, jnp.bfloat16)),
            axis,
        )
        inside, total = (start, start)
        for k in range(size):
            passed = k < here
            total = combine(
                total, jax.tree.map(lambda part, own: part[k].astype(own.dtype), pieces, value)
            )
            inside = jax.tree.map(lambda new, old: jnp.where(passed, new, old), total, inside)
        before = combine(inside, before)
    return before


def split_up(value, dim, size):
    shape = value.shape
    parts = value.reshape(*shape[:dim], size, shape[dim] // size, *shape[dim + 1 :])
    return jnp.moveaxis(parts, dim, 0)


def laid_out(parts, dim):
    shape = list(parts.shape[1:])
    shape[dim] *= parts.shape[0]
    return jnp.moveaxis(parts, 0, dim).reshape(shape)


def turned_blocks(parts, axes, order):
    shape = [lax.axis_size(a) for a in axes]
    parts = parts.reshape(*shape, *parts.shape[1:])
    for k in order:
        parts = lax.all_to_all(parts, axes[k], split_axis=k, concat_axis=k, tiled=True)
    return parts.reshape(-1, *parts.shape[len(axes) :])


def two_step_exchange(value, groups, order, split_dim, concat_dim):
    size = lax.axis_size(groups[0]) * lax.axis_size(groups[1])
    parts = split_up(value, split_dim, size)
    return laid_out(turned_blocks(parts, groups, order), concat_dim)


def copy_for_each(value, axis):
    size = lax.axis_size(axis)
    return lax.all_to_all(
        jnp.broadcast_to(value[None], (size, *value.shape)), axis, 0, 0, tiled=True
    )


def gathered_copies(value, axis, dim):
    parts = copy_for_each(value, axis)
    return laid_out(parts, dim)


def sent_together(arrays, axis, dim, along):
    ends, at = ([], 0)
    for a in arrays[:-1]:
        at += a.shape[along]
        ends.append(at)
    both = jnp.concatenate(arrays, axis=along)
    return tuple(jnp.split(lax.all_gather(both, axis, axis=dim, tiled=True), ends, axis=along))


def head_norm(tensor, gain_rows):
    mean_square = jnp.mean(tensor * tensor, axis=-1, keepdims=True)
    return tensor * lax.rsqrt(mean_square + epsilon) * gain_rows


def log_decay_values(decay_preactivation, channel_decay_bias, added_log_decay):
    number_of_heads = added_log_decay.shape[0]
    row_count = decay_preactivation.shape[0]
    logits = decay_preactivation.astype(jnp.float32) + channel_decay_bias[None, :]
    baseline_log_decay = (jax.nn.log_sigmoid(logits) / temper).reshape(
        row_count, number_of_heads, -1
    )
    return baseline_log_decay + jnp.transpose(added_log_decay)[:, :, None]


def combine_states(earlier, latter):
    return (earlier[0] * latter[0], latter[0][..., None] * earlier[1] + latter[1])


def mixer_heads(
    first_batch_queries,
    first_batch_keys,
    first_batch_values,
    output_gate_preactivation,
    decay_preactivation,
    channel_decay_bias,
    added_log_decay,
    head_norm_gain,
):
    number_of_heads = added_log_decay.shape[0]
    row_count = first_batch_queries.shape[0]
    key_channel_width = first_batch_queries.shape[1] // number_of_heads
    value_width = first_batch_values.shape[1] // number_of_heads
    block_count = row_count // BLOCK

    def split_into_blocks(tensor, width):
        shaped = tensor.astype(jnp.float32).reshape(block_count, BLOCK, number_of_heads, width)
        return shaped.transpose(0, 2, 1, 3)

    queries = split_into_blocks(first_batch_queries, key_channel_width)
    keys_all = split_into_blocks(first_batch_keys, key_channel_width)
    values = split_into_blocks(first_batch_values, value_width)
    decay_factors = split_into_blocks(
        log_decay_values(decay_preactivation, channel_decay_bias, added_log_decay),
        key_channel_width,
    )
    running_state = jnp.cumsum(decay_factors, axis=2)
    block_number_total = running_state[:, :, -1, :]
    query_decayed = queries * jnp.exp(running_state)
    key_raised = keys_all * jnp.exp(-running_state)
    lower_mask = jnp.tril(jnp.ones((BLOCK, BLOCK), bool))
    attention_scores = jnp.einsum("nhqd,nhkd->nhqk", query_decayed, key_raised)
    attention_scores = jnp.where(lower_mask, attention_scores, 0.0)
    within_block = jnp.einsum("nhqk,nhkv->nhqv", attention_scores, values)
    updates = jnp.einsum(
        "nhkd,nhkv->nhdv",
        keys_all * jnp.exp(block_number_total[:, :, None, :] - running_state),
        values,
    )

    def carry_blocks(carry_state, inputs):
        state_update, total_log = inputs
        return (jnp.exp(total_log)[..., None] * carry_state + state_update, carry_state)

    zero_state = jnp.zeros((number_of_heads, key_channel_width, value_width), jnp.float32)
    device_state, before = lax.scan(carry_blocks, zero_state, (updates, block_number_total))
    device_decay = jnp.exp(jnp.sum(block_number_total, axis=0))
    identity = (jnp.ones((number_of_heads, key_channel_width), jnp.float32), zero_state)
    _, incoming = carried_in((device_decay, device_state), EP, combine_states, identity)
    lead_in = jnp.exp(jnp.cumsum(block_number_total, axis=0) - block_number_total)
    states = before + lead_in[..., None] * incoming[None]
    carried = jnp.einsum("nhqd,nhdv->nhqv", query_decayed, states)
    head_values = (
        (within_block + carried)
        .transpose(0, 2, 1, 3)
        .reshape(row_count, number_of_heads, value_width)
    )
    gate_rows = jax.nn.silu(output_gate_preactivation.astype(jnp.float32)).reshape(
        row_count, number_of_heads, value_width
    )
    gated_heads = (
        head_norm(head_values, head_norm_gain.reshape(number_of_heads, value_width)) * gate_rows
    )
    return gated_heads.reshape(row_count, number_of_heads * value_width).astype(jnp.bfloat16)


def expert_slots(route_rows, experts, capacity):
    flat_ids = route_rows.reshape(-1)
    targets = jnp.arange(experts, dtype=jnp.int32)
    onehot = (flat_ids[:, None] == targets[None, :]).astype(jnp.int32)
    earlier = jnp.cumsum(onehot, axis=0) - onehot
    return flat_ids * capacity + jnp.sum(earlier * onehot, axis=1)


def slot_owner(slot_ids, slot_count, top_count):
    matches = slot_ids[None, :] == jnp.arange(slot_count, dtype=jnp.int32)[:, None]
    token_ids = jnp.arange(slot_ids.shape[0], dtype=jnp.int32) // top_count
    return jnp.sum(jnp.where(matches, token_ids[None, :] + 1, 0), axis=1) - 1


def fill_slots(source_rows, owners):
    picked_rows = jnp.take(source_rows, jnp.maximum(owners, 0), axis=0)
    return jnp.where((owners >= 0)[:, None], picked_rows, jnp.zeros((), jnp.bfloat16))


def paired_rows(tensor, factor):
    return tensor.reshape(tensor.shape[0] // factor, tensor.shape[1] * factor)


def paired_product(section, weight, factor, own_width):
    row_count = section.shape[0]
    pieces = section.reshape(row_count, -1, factor, own_width)
    products = [
        jnp.dot(
            pieces[:, :, which, :].reshape(row_count, -1),
            weight,
            preferred_element_type=jnp.float32,
        )
        for which in range(factor)
    ]
    return jnp.stack(products, axis=1)


def local(
    first_batch_queries,
    first_batch_keys,
    first_batch_values,
    output_gate_preactivation,
    decay_preactivation,
    channel_decay_bias,
    added_log_decay,
    head_norm_gain,
    attention_output_weight,
    second_batch_rows,
    expert_norm_gain,
    routed_expert_index,
    router_chosen_scores,
    expert_gate_weight,
    expert_up_weight,
    expert_down_weight,
    shared_gate_weight,
    shared_up_weight,
    shared_down_weight,
):
    mixed_heads = mixer_heads(
        first_batch_queries,
        first_batch_keys,
        first_batch_values,
        output_gate_preactivation,
        decay_preactivation,
        channel_decay_bias,
        added_log_decay,
        head_norm_gain,
    )
    experts = lax.axis_size(EP)
    tokens, top_count = routed_expert_index.shape
    capacity = tokens * top_count * 3 // (2 * experts)
    slot_count = experts * capacity
    model_width = second_batch_rows.shape[1]
    features = second_batch_rows.astype(jnp.float32)
    normed = features * lax.rsqrt(jnp.mean(features * features, axis=1, keepdims=True) + epsilon)
    normed = (normed * expert_norm_gain[None, :]).astype(jnp.bfloat16)
    slot_ids = expert_slots(routed_expert_index, experts, capacity)
    owners = slot_owner(slot_ids, slot_count, top_count)
    gate_weight = expert_gate_weight[0]
    up_weight = expert_up_weight[0]
    down_weight = expert_down_weight[0]
    columns = model_width // lax.axis_size("tp")
    own_columns = lax.dynamic_slice_in_dim(normed, lax.axis_index("tp") * columns, columns, 1)
    outgoing = fill_slots(own_columns, owners).reshape(experts, capacity, columns)
    arrived = two_step_exchange(outgoing, ("ep_0", "ep_1"), (1, 0), 0, 0)
    flat_columns = arrived.reshape(slot_count, columns)
    section = gathered_copies(flat_columns, "tp", 1)
    gate_value = jnp.dot(section, gate_weight, preferred_element_type=jnp.float32)
    up_value = jnp.dot(section, up_weight, preferred_element_type=jnp.float32)
    routed_hidden = (jax.nn.silu(gate_value) * up_value).astype(jnp.bfloat16)
    hidden_width = routed_hidden.shape[1]
    shared_gate_value = jnp.dot(normed, shared_gate_weight, preferred_element_type=jnp.float32)
    shared_up_value = jnp.dot(normed, shared_up_weight, preferred_element_type=jnp.float32)
    shared_hidden = (jax.nn.silu(shared_gate_value) * shared_up_value).astype(jnp.bfloat16)
    shared_width = shared_hidden.shape[1]
    shared_factor = hidden_width // shared_width
    shared_paired = paired_rows(shared_hidden, shared_factor)
    mixer_total = jnp.dot(
        gathered_copies(mixed_heads, "tp", 1),
        attention_output_weight,
        preferred_element_type=jnp.float32,
    )
    routed_section, shared_section = sent_together((routed_hidden, shared_paired), "tp", 1, 0)
    routed_part = jnp.dot(routed_section, down_weight, preferred_element_type=jnp.float32)
    shared_part = paired_product(shared_section, shared_down_weight, shared_factor, shared_width)
    shared_total = shared_part.reshape(tokens, -1)
    token_mixed = mixer_total.astype(jnp.bfloat16)
    routed_output = routed_part.astype(jnp.bfloat16).reshape(experts, capacity, -1)
    returned = two_step_exchange(routed_output, ("ep_0", "ep_1"), (1, 0), 0, 0).reshape(
        slot_count, -1
    )
    picked = jnp.take(returned, slot_ids, axis=0).astype(jnp.float32).reshape(tokens, top_count, -1)
    weights = (
        routed_scale * router_chosen_scores / jnp.sum(router_chosen_scores, axis=1, keepdims=True)
    )
    channel_mixed = (jnp.sum(weights[:, :, None] * picked, axis=1) + shared_total).astype(
        jnp.bfloat16
    )
    return (token_mixed, channel_mixed)


def solution(mesh):
    torus = Mesh(mesh.devices.reshape(16, 2, mesh.shape["tp"]), ("ep_0", "ep_1", "tp"))
    return jax.shard_map(
        local,
        mesh=torus,
        in_specs=(
            P(EP, "tp"),
            P(EP, "tp"),
            P(EP, "tp"),
            P(EP, "tp"),
            P(EP, "tp"),
            P("tp"),
            P("tp", EP),
            P("tp"),
            P(None, "tp"),
            P(EP, None),
            P(),
            P(EP, None),
            P(EP, None),
            P(EP, None, "tp"),
            P(EP, None, "tp"),
            P(EP, None, "tp"),
            P(None, "tp"),
            P(None, "tp"),
            P(None, "tp"),
        ),
        out_specs=(P(EP, "tp"), P(EP, "tp")),
        check_vma=False,
    )
```

profile of v0, /device:TPU:1, one launch (start us, length us, event | category | flops | bytes accessed | tf_op | source)
XLA Modules:
  0.0 212.2 jit_solution(3611692390714834288)
XLA Ops:
  7.2 0.9 copy.149
  8.3 0.9 reduce-window.6
  9.7 1.2 fusion.23
  11.0 1.2 fusion.25
  12.1 1.9 gather_fusion
  14.7 10.3 %all_to_all.30 = bf16[16,2,1,18,128]{4,0,3,2,1:T(8,128)(2,1)S(1)} all-to-all(bf16[16,2,1,18,128]{4,0,3,2,1:T(8,128)(2,1)S(1)} %copy.154), channel_id=1, replica_groups=mesh['ep_0'=16,'ep_1'=2,'tp'=16] {'ep_1'}, dimensions={1} | all-to-all | bytes 294912 | tf_op jit(solution)/shard_map/all_to_all | solution.py:75
  25.1 21.6 %all_to_all.31 = bf16[16,2,1,18,128]{4,1,3,2,0:T(2,128)(2,1)S(1)} all-to-all(bf16[16,2,1,18,128]{4,1,3,2,0:T(2,128)(2,1)S(1)} %copy.155), channel_id=1, replica_groups=mesh['ep_0'=16,'ep_1'=2,'tp'=16] {'ep_0'}, dimensions={0} | all-to-all | bytes 294912 | tf_op jit(solution)/shard_map/all_to_all | solution.py:75
  46.8 1.8 broadcast_in_dim.131
  48.7 6.9 %all-to-all-start.3 = ((bf16[16,576,128]{2,1,0:T(8,128)(2,1)}), bf16[16,576,128]{2,1,0:T(8,128)(2,1)}, u32[]{:S(2)}, u32[]{:S(2)}) async-start(bf16[16,576,128]{2,1,0:T(8,128)(2,1)} %broadcast_in_dim.131), calls=%async_computation.3 | async-start | bytes 4718592 | tf_op jit(solution)/shard_map/all_to_all | solution.py:87
  56.4 26.7 %all-to-all-done.3 = bf16[16,576,128]{2,1,0:T(8,128)(2,1)} async-done(((bf16[16,576,128]{2,1,0:T(8,128)(2,1)}), bf16[16,576,128]{2,1,0:T(8,128)(2,1)}, u32[]{:S(2)}, u32[]{:S(2)}) %all-to-all-start.3) | async-done | bytes 2359328 | tf_op jit(solution)/shard_map/all_to_all | solution.py:87
  83.1 2.5 %fusion.6 = f32[576,256]{1,0:T(8,128)S(1)} fusion(bf16[1,2048,256]{2,1,0:T(8,128)(2,1)S(1)} %copy-done, bf16[16,576,128]{2,1,0:T(8,128)(2,1)} %all-to-all-done.3), kind=kOutput, calls=%fused_computation.11 | convolution fusion | flops 603979776 | bytes 3997696 | tf_op jit(solution)/shard_map/dot_general | solution.py:279
  85.7 2.5 %fusion.13 = bf16[576,256]{1,0:T(8,128)(2,1)S(1)} fusion(bf16[1,2048,256]{2,1,0:T(8,128)(2,1)S(1)} %copy-done.15, f32[576,256]{1,0:T(8,128)S(1)} %fusion.6, bf16[16,576,128]{2,1,0:T(8,128)(2,1)} %all-to-all-done.3), kind=kOutput, calls=%fused_computation.16 | convolution fusion | flops 604864512 | bytes 4292608 | tf_op jit(solution)/shard_map/dot_general | solution.py:280
  88.2 0.8 pad_maximum_fusion
  89.8 0.5 while.13
  90.3 8.0 %all-gather.2 = bf16[2,65,128]{2,1,0:T(8,128)(2,1)S(1)} all-gather(bf16[1,65,128]{2,1,0:T(8,128)(2,1)S(1)} %maximum_bitcast_fusion), channel_id=2, replica_groups=mesh['ep_0'=16,'ep_1'=2,'tp'=16] {'ep_1'}, dimensions={0}, use_global_device_ids=true | all-gather | bytes 49920 | tf_op jit(solution)/shard_map/all_gather | solution.py:30
  98.5 26.7 %all-gather.3 = bf16[16,65,128]{2,1,0:T(8,128)(2,1)S(1)} all-gather(bf16[1,65,128]{2,1,0:T(8,128)(2,1)S(1)} %maximum_bitcast_fusion.1), channel_id=3, replica_groups=mesh['ep_0'=16,'ep_1'=2,'tp'=16] {'ep_0'}, dimensions={0}, use_global_device_ids=true | all-gather | bytes 282880 | tf_op jit(solution)/shard_map/all_gather | solution.py:30
  125.9 0.4 multiply_reduce_fusion.1
  126.6 1.1 broadcast_in_dim.79
  127.7 3.7 %all-to-all-start = ((bf16[16,256,128]{1,2,0:T(8,128)(2,1)}), bf16[16,256,128]{1,2,0:T(8,128)(2,1)S(1)}, u32[]{:S(2)}, u32[]{:S(2)}) async-start(bf16[16,256,128]{1,2,0:T(8,128)(2,1)} %broadcast_in_dim.79), calls=%async_computation | async-start | bytes 2097152 | tf_op jit(solution)/shard_map/all_to_all | solution.py:87
  132.1 11.5 %all-to-all-done = bf16[16,256,128]{1,2,0:T(8,128)(2,1)S(1)} async-done(((bf16[16,256,128]{1,2,0:T(8,128)(2,1)}), bf16[16,256,128]{1,2,0:T(8,128)(2,1)S(1)}, u32[]{:S(2)}, u32[]{:S(2)}) %all-to-all-start) | async-done | bytes 1048608 | tf_op jit(solution)/shard_map/all_to_all | solution.py:87
  143.6 1.1 convolution_convert_fusion
  144.7 27.2 %all-gather.6.cloned.1.call-done = bf16[600,4096]{1,0:T(8,128)(2,1)} async-done(((bf16[600,256]{1,0:T(8,128)(2,1)}), bf16[600,4096]{1,0:T(8,128)(2,1)}) %all-gather.6.cloned.1.call-update) | async-done | bytes 4915216 | tf_op jit(solution)/shard_map/all_gather | solution.py:103
  171.9 4.1 %fusion.16 = bf16[576,128]{1,0:T(8,128)(2,1)S(1)} fusion(bf16[600,4096]{1,0:T(8,128)(2,1)} %all-gather.6.cloned.1.call-done, bf16[1,4096,128]{2,1,0:T(8,128)(2,1)} %param.36), kind=kOutput, calls=%fused_computation.17 | convolution fusion | flops 604053504 | bytes 5914624 | tf_op jit(solution)/shard_map/dot_general | solution.py:295
  176.1 5.1 %all_to_all.32 = bf16[16,2,1,18,128]{4,0,3,2,1:T(8,128)(2,1)S(1)} all-to-all(bf16[16,2,1,18,128]{4,0,3,2,1:T(8,128)(2,1)S(1)} %copy.159), channel_id=1, replica_groups=mesh['ep_0'=16,'ep_1'=2,'tp'=16] {'ep_1'}, dimensions={1} | all-to-all | bytes 294912 | tf_op jit(solution)/shard_map/all_to_all | solution.py:75
  181.1 0.8 copy.160
  181.9 8.8 %all-to-all-start.5 = ((bf16[16,2,1,18,128]{4,1,3,2,0:T(2,128)(2,1)}), bf16[16,2,1,18,128]{4,1,3,2,0:T(2,128)(2,1)S(1)}, u32[]{:S(2)}, u32[]{:S(2)}) async-start(bf16[16,2,1,18,128]{4,1,3,2,0:T(2,128)(2,1)} %copy.160), calls=%async_computation.5 | async-start | bytes 294912 | tf_op jit(solution)/shard_map/all_to_all | solution.py:75
  190.7 0.4 reshape.763
  191.1 2.3 %slice_reduce_fusion.3 = (bf16[24,16,64]{2,1,0:T(8,128)(2,1)S(1)}, bf16[24,16,64]{2,1,0:T(8,128)(2,1)S(1)}, bf16[24,16,64]{2,1,0:T(8,128)(2,1)S(1)}, bf16[24,16,64]{2,1,0:T(8,128)(2,1)S(1)}) fusion(bf16[24,16,4,64]{3,2,1,0:T(4,128)(2,1)S(1)} %reshape.763), kind=kLoop, calls=%fused_computation.42 | loop fusion | bytes 393216 | tf_op jit(solution)/shard_map/slice | solution.py:220
  194.6 8.3 %all-to-all-done.5 = bf16[16,2,1,18,128]{4,1,3,2,0:T(2,128)(2,1)S(1)} async-done(((bf16[16,2,1,18,128]{4,1,3,2,0:T(2,128)(2,1)}), bf16[16,2,1,18,128]{4,1,3,2,0:T(2,128)(2,1)S(1)}, u32[]{:S(2)}, u32[]{:S(2)}) %all-to-all-start.5) | async-done | bytes 147488 | tf_op jit(solution)/shard_map/all_to_all | solution.py:75
  203.0 1.4 gather_fusion.1
  204.4 0.3 multiply_reduce_fusion
  204.7 0.6 add_convert_fusion
  (132 shorter events, 6.7 us)
Async XLA Ops:
  7.2 75.9 %copy-start = (bf16[1,2048,256]{2,1,0:T(8,128)(2,1)S(1)}, bf16[1,2048,256]{2,1,0:T(8,128)(2,1)}, u32[]{:S(2)}) copy-start(bf16[1,2048,256]{2,1,0:T(8,128)(2,1)} %param.34) | copy-start | bytes 3145732
  48.7 7.0 %copy-start.3 = (bf16[2048,64]{0,1:T(8,128)(2,1)S(1)}, bf16[2048,64]{0,1:T(8,128)(2,1)}, u32[]{:S(2)}) copy-start(bf16[2048,64]{0,1:T(8,128)(2,1)} %param.37) | copy-start | bytes 786436
  48.7 7.3 %copy-start.4 = (bf16[2048,64]{0,1:T(8,128)(2,1)S(1)}, bf16[2048,64]{0,1:T(8,128)(2,1)}, u32[]{:S(2)}) copy-start(bf16[2048,64]{0,1:T(8,128)(2,1)} %param.38) | copy-start | bytes 786436
  48.7 34.4 %all-to-all-start.3 = ((bf16[16,576,128]{2,1,0:T(8,128)(2,1)}), bf16[16,576,128]{2,1,0:T(8,128)(2,1)}, u32[]{:S(2)}, u32[]{:S(2)}) async-start(bf16[16,576,128]{2,1,0:T(8,128)(2,1)} %broadcast_in_dim.131), calls=%async_computation.3 | async-start | bytes 4718592 | tf_op jit(solution)/shard_map/all_to_all | solution.py:87
  55.6 116.3 %all-gather.6.cloned.1.call-start = ((), (), s32[]{:S(2)}) async-start(), calls=%async_computation.6 | async-start | bytes 5222400 | tf_op jit(solution)/shard_map/all_gather | solution.py:103
  83.1 2.5 %copy-start.15 = (bf16[1,2048,256]{2,1,0:T(8,128)(2,1)S(1)}, bf16[1,2048,256]{2,1,0:T(8,128)(2,1)}, u32[]{:S(2)}) copy-start(bf16[1,2048,256]{2,1,0:T(8,128)(2,1)} %param.35) | copy-start | bytes 3145732
  85.6 3.4 %copy-start.7 = (bf16[256,64]{0,1:T(8,128)(2,1)S(1)}, bf16[256,64]{0,1:T(8,128)(2,1)}, u32[]{:S(2)}) copy-start(bf16[256,64]{0,1:T(8,128)(2,1)} %param.25) | copy-start | bytes 98308
  85.7 3.4 %copy-start.12 = (f32[1,256]{1,0:T(1,128)S(1)}, f32[1,256]{1,0:T(1,128)}, u32[]{:S(2)}) copy-start(f32[1,256]{1,0:T(1,128)} %param.27) | copy-start | bytes 3076
  85.7 3.4 %copy-start.13 = (f32[64]{0:T(128)S(1)}, f32[64]{0:T(128)}, u32[]{:S(2)}) copy-start(f32[64]{0:T(128)} %param.26) | copy-start | bytes 772
  85.7 3.6 %copy-start.8 = (bf16[256,64]{0,1:T(8,128)(2,1)S(1)}, bf16[256,64]{0,1:T(8,128)(2,1)}, u32[]{:S(2)}) copy-start(bf16[256,64]{0,1:T(8,128)(2,1)} %param.22) | copy-start | bytes 98308
  85.7 3.9 %copy-start.5 = (bf16[256,128]{1,0:T(8,128)(2,1)S(1)}, bf16[256,128]{1,0:T(8,128)(2,1)}, u32[]{:S(2)}) copy-start(bf16[256,128]{1,0:T(8,128)(2,1)} %param.23) | copy-start | bytes 196612
  88.2 37.0 %copy-start.9 = (bf16[256,64]{0,1:T(8,128)(2,1)S(1)}, bf16[256,64]{0,1:T(8,128)(2,1)}, u32[]{:S(2)}) copy-start(bf16[256,64]{0,1:T(8,128)(2,1)} %param.21) | copy-start | bytes 98308
  89.2 37.2 %copy-start.6 = (bf16[256,128]{1,0:T(8,128)(2,1)S(1)}, bf16[256,128]{1,0:T(8,128)(2,1)}, u32[]{:S(2)}) copy-start(bf16[256,128]{1,0:T(8,128)(2,1)} %param.24) | copy-start | bytes 196612
  89.2 37.2 %copy-start.14 = (f32[128]{0:T(128)S(1)}, f32[128]{0:T(128)}, u32[]{:S(2)}) copy-start(f32[128]{0:T(128)} %param.28) | copy-start | bytes 1540
  125.8 5.6 %copy-start.10 = (s32[96,4]{0,1:T(4,128)S(1)}, s32[96,4]{0,1:T(4,128)}, u32[]{:S(2)}) copy-start(s32[96,4]{0,1:T(4,128)} %param.32) | copy-start | bytes 4612
  125.9 5.8 %copy-start.11 = (f32[96,4]{0,1:T(4,128)S(1)}, f32[96,4]{0,1:T(4,128)}, u32[]{:S(2)}) copy-start(f32[96,4]{0,1:T(4,128)} %param.33) | copy-start | bytes 4612
  125.9 17.7 %copy-start.2 = (bf16[2048,128]{1,0:T(8,128)(2,1)S(1)}, bf16[2048,128]{1,0:T(8,128)(2,1)}, u32[]{:S(2)}) copy-start(bf16[2048,128]{1,0:T(8,128)(2,1)} %param.29) | copy-start | bytes 1572868
  127.7 15.9 %all-to-all-start = ((bf16[16,256,128]{1,2,0:T(8,128)(2,1)}), bf16[16,256,128]{1,2,0:T(8,128)(2,1)S(1)}, u32[]{:S(2)}, u32[]{:S(2)}) async-start(bf16[16,256,128]{1,2,0:T(8,128)(2,1)} %broadcast_in_dim.79), calls=%async_computation | async-start | bytes 2097152 | tf_op jit(solution)/shard_map/all_to_all | solution.py:87
  171.9 18.8 %slice-start = ((bf16[600,4096]{1,0:T(8,128)(2,1)}), bf16[24,4096]{1,0:T(8,128)(2,1)S(1)}, s32[]{:S(2)}) async-start(bf16[600,4096]{1,0:T(8,128)(2,1)} %all-gather.6.cloned.1.call-done), calls=%async_computation.7 | async-start | bytes 393216 | tf_op jit(solution)/shard_map/split | solution.py:103
  175.9 17.5 %copy-start.1 = (bf16[1024,128]{1,0:T(8,128)(2,1)S(1)}, bf16[1024,128]{1,0:T(8,128)(2,1)}, u32[]{:S(2)}) copy-start(bf16[1024,128]{1,0:T(8,128)(2,1)} %param.39) | copy-start | bytes 786436
  181.9 21.0 %all-to-all-start.5 = ((bf16[16,2,1,18,128]{4,1,3,2,0:T(2,128)(2,1)}), bf16[16,2,1,18,128]{4,1,3,2,0:T(2,128)(2,1)S(1)}, u32[]{:S(2)}, u32[]{:S(2)}) async-start(bf16[16,2,1,18,128]{4,1,3,2,0:T(2,128)(2,1)} %copy.160), calls=%async_computation.5 | async-start | bytes 294912 | tf_op jit(solution)/shard_map/all_to_all | solution.py:75
Sparse Core Ops, SparseCore 0:
  89.1 82.7 all-gather.5
where the time goes:
time: 214 us; the launch traced here: 212 us
  waiting for transfers between devices  73.7 us (34%)
  blocking collectives  71.6 us (33%)
  starting transfers between devices  19.4 us (9%)
  between operations  14.8 us (7%)
  local copies, waits for them, and re-layouts  13.8 us (6%)
  matrix products  12.1 us (6%)
  other arithmetic  6.79 us (3%)
    all_to_all x2, waiting for transfers between devices, copy_for_each(): lax.all_to_all(jnp.broadcast_to(value[None], (size, *value.shape)), axis,...  38.2 us
    all_to_all x3, blocking collectives, turned_blocks(): lax.all_to_all(parts, axes[k], split_axis=k, concat_axis=k, tiled=True)  37 us
    all_gather x2, blocking collectives, collected_together(): both, at, found = (lax.all_gather(jnp.concatenate(lines), axis), 0, {})  34.7 us
    all_gather x1, waiting for transfers between devices, sent_together(): lax.all_gather(both, axis, axis=dim, tiled=True)  27.2 us
    all_to_all x2, starting transfers between devices, copy_for_each(): lax.all_to_all(jnp.broadcast_to(value[None], (size, *value.shape)), axis,...  10.6 us
    all_to_all x1, starting transfers between devices, turned_blocks(): lax.all_to_all(parts, axes[k], split_axis=k, concat_axis=k, tiled=True)  8.76 us
    all_to_all x1, waiting for transfers between devices, turned_blocks(): lax.all_to_all(parts, axes[k], split_axis=k, concat_axis=k, tiled=True)  8.33 us
  transfers between devices with their start and end apart: 4, of which 4 were waited for; matrix products, arithmetic and copies ran while one was open for 5% of the time, Pallas kernels for 0%

commit v1 on v0

v1 whole, which is shorter than its diff:
```python
from collections import namedtuple
from typing import NamedTuple

import jax
import jax.numpy as jnp
from jax import lax
from jax.experimental import pallas as pl
from jax.experimental.pallas import tpu as pltpu
from jax.sharding import Mesh
from jax.sharding import PartitionSpec as P

MESH = pl.DeviceIdType.MESH
F32 = jnp.float32
BF16 = jnp.bfloat16

EPS = 1e-06
TEMPER = 16.0
ROUTED_SCALE = 2.5
BLOCK = 64
RING = 4
EXPERTS = 32
MAIN = 16
LEFT = 2
MAIN_ROWS = EXPERTS * MAIN
SLOTS = EXPERTS * (MAIN + LEFT)
CHUNKS = 4
PER_CHUNK = EXPERTS // CHUNKS
CHUNK_MAIN = PER_CHUNK * MAIN
CHUNK = PER_CHUNK * (MAIN + LEFT)
TOP = 80
TOK_A = 256
TOK_B = 96
COLS = 128
HEAD_K = 64
MIX_ROWS = TOK_A + TOK_B // 2


def nn(a, b):
    return lax.dot_general(a, b, (((1,), (0,)), ((), ())), preferred_element_type=F32)


def nt(a, b):
    return lax.dot_general(a, b, (((1,), (1,)), ((), ())), preferred_element_type=F32)


def tn(a, b):
    return lax.dot_general(a, b, (((0,), (0,)), ((), ())), preferred_element_type=F32)


def silu(a):
    return a / (1.0 + jnp.exp(-a))


def sums_of(value, picks):
    high = value.astype(BF16)
    rest = value - high.astype(F32)
    middle = rest.astype(BF16)
    low = (rest - middle.astype(F32)).astype(BF16)
    return nn(high, picks) + nn(middle, picks) + nn(low, picks)


def as_column(row):
    return jnp.broadcast_to(row, (128, row.shape[1])).T


def split_rows(start, stop):
    return pl.ds(start, stop - start)


class Inputs(NamedTuple):
    q: object
    k: object
    v: object
    og: object
    dec: object
    bias: object
    added: object
    hgain: object
    wo: object
    rows: object
    egain: object
    idx: object
    scores: object
    wg: object
    wu: object
    wd: object
    sg: object
    su: object
    sd: object


def layer_kernel(zs, given, token_mixed, channel_mixed, r):
    z, c = lax.axis_index("z"), lax.axis_index("c")
    y, x = lax.axis_index("y"), lax.axis_index("x")
    experts = zs * 2
    me = z * 2 + c
    tp = y * RING + x

    def turn(a, d):
        return lax.rem(a + d + RING, RING)

    partner = (z, 1 - c, y, x)
    x_up, x_down = (z, c, y, turn(x, 1)), (z, c, y, turn(x, -1))
    y_up, y_down = (z, c, turn(y, 1), x), (z, c, turn(y, -1), x)

    def ep_device(e):
        return (e // 2, lax.rem(e, 2), y, x)

    class Load:
        count = 0

        def __init__(self, source, target):
            self.copy = pltpu.make_async_copy(source, target, r.load_sem.at[Load.count])
            Load.count += 1
            self.copy.start()

    rows_loads = [
        Load(given.rows, r.rows), Load(given.egain, r.egain),
        Load(given.idx, r.idx), Load(given.scores, r.scores),
    ]
    mixer_loads = [
        Load(given.dec, r.dec), Load(given.bias, r.bias), Load(given.added, r.added),
        Load(given.k, r.k), Load(given.v, r.v), Load(given.q, r.q),
        Load(given.og, r.og), Load(given.hgain, r.hgain),
    ]
    shared_loads = [Load(given.sg, r.sgu.at[pl.ds(0, 64)]), Load(given.su, r.sgu.at[pl.ds(64, 64)])]
    gate_loads = [Load(given.wg.at[0], r.wg), Load(given.wu.at[0], r.wu)]
    down_loads = [Load(given.wd.at[y], r.wd1.at[y]), Load(given.wd.at[:, x], r.wd2.at[x])]
    last_loads = [
        Load(given.wo, r.wo), Load(given.sd, r.sd.at[:, 0]), Load(given.sd, r.sd.at[:, 1]),
    ]

    def loaded(group):
        for item in group:
            item.copy.wait()

    r.chip_in[...] = jnp.zeros_like(r.chip_in)
    r.chip_log_in[...] = jnp.zeros_like(r.chip_log_in)
    barrier = pltpu.get_barrier_semaphore()

    def greet(d, carry):
        pl.semaphore_signal(
            barrier, inc=1, device_id=ep_device(lax.rem(me + d, experts)), device_id_type=MESH
        )
        return carry

    lax.fori_loop(1, experts, greet, 0)
    for who in (x_up, x_down, y_up, y_down):
        pl.semaphore_signal(barrier, inc=1, device_id=who, device_id_type=MESH)

    loaded(rows_loads)
    features = r.rows[...].astype(F32)
    scale = lax.rsqrt(jnp.mean(features * features, axis=1, keepdims=True) + EPS)
    r.normed[...] = (features * scale * r.egain[...]).astype(BF16)

    expert_row = lax.broadcasted_iota(jnp.int32, (EXPERTS, TOK_B), 0)
    idx = r.idx[...]
    scores = r.scores[...]
    weights = ROUTED_SCALE * scores / jnp.sum(scores, axis=0, keepdims=True)
    named = jnp.zeros((EXPERTS, TOK_B), F32)
    share = jnp.zeros((EXPERTS, TOK_B), F32)
    for k in range(4):
        hit = idx[k : k + 1] == expert_row
        named = jnp.where(hit, 1.0, named)
        share = jnp.where(hit, weights[k : k + 1], share)
    before = (
        lax.broadcasted_iota(jnp.int32, (TOK_B, TOK_B), 0)
        < lax.broadcasted_iota(jnp.int32, (TOK_B, TOK_B), 1)
    )
    rank = nn(named.astype(BF16), jnp.where(before, 1.0, 0.0).astype(BF16))
    rank = jnp.where(named > 0.0, rank, 100.0).astype(BF16)

    def slot_parts(q):
        whole = q < MAIN_ROWS
        owner = jnp.where(whole, q // MAIN, (q - MAIN_ROWS) // LEFT)
        place = jnp.where(whole, lax.rem(q, MAIN), MAIN + lax.rem(q, LEFT))
        return owner, place

    owner, place = slot_parts(lax.broadcasted_iota(jnp.int32, (SLOTS, EXPERTS), 0))
    spread = owner == lax.broadcasted_iota(jnp.int32, (SLOTS, EXPERTS), 1)
    picks = nn(jnp.where(spread, 1.0, 0.0).astype(BF16), rank)
    picks = jnp.where(picks == place[:, :1].astype(F32), 1.0, 0.0).astype(BF16)
    own_columns = r.normed[:, pl.ds(pl.multiple_of(tp * COLS, COLS), COLS)]
    slots = nn(picks, own_columns)
    r.out_main[...] = slots[:MAIN_ROWS].astype(BF16)

    def store_left(ref, value):
        value = value.astype(BF16)
        for e in range(EXPERTS):
            ref[e] = value[LEFT * e : LEFT * e + LEFT]

    store_left(r.out_left, slots[MAIN_ROWS:])

    owner, place = slot_parts(lax.broadcasted_iota(jnp.int32, (EXPERTS, SLOTS), 1))
    spread = owner == lax.broadcasted_iota(jnp.int32, (EXPERTS, SLOTS), 0)
    spread = jnp.where(spread, 1.0, 0.0).astype(BF16)
    here = tn(rank, spread) == place[:1].astype(F32)
    share_high = share.astype(BF16)
    share_low = (share - share_high.astype(F32)).astype(BF16)
    r.mix_high[...] = jnp.where(here, tn(share_high, spread), 0.0).astype(BF16)
    r.mix_low[...] = jnp.where(here, tn(share_low, spread), 0.0).astype(BF16)

    loaded(mixer_loads)
    logits = r.dec[...].astype(F32) + as_column(r.bias[...])[:, :1]
    log_gate = jnp.minimum(logits, 0.0) - jnp.log1p(jnp.exp(-jnp.abs(logits)))
    decay = log_gate / TEMPER + r.added[...]
    row = lax.broadcasted_iota(jnp.int32, (TOK_A, TOK_A), 0)
    col = lax.broadcasted_iota(jnp.int32, (TOK_A, TOK_A), 1)
    tri = jnp.where((row // BLOCK == col // BLOCK) & (row <= col), 1.0, 0.0).astype(BF16)
    running = sums_of(decay, tri)
    queries = r.q[...].astype(F32) * jnp.exp(running)
    keys = r.k[...].astype(F32)
    raised = (keys * jnp.exp(-running)).astype(BF16)
    lower = lax.broadcasted_iota(jnp.int32, (BLOCK, BLOCK), 1) <= lax.broadcasted_iota(
        jnp.int32, (BLOCK, BLOCK), 0
    )
    state = jnp.zeros((HEAD_K, COLS), F32)
    lead = jnp.zeros((HEAD_K, 1), F32)
    for b in range(TOK_A // BLOCK):
        at = slice(b * BLOCK, (b + 1) * BLOCK)
        total = running[:, (b + 1) * BLOCK - 1 : (b + 1) * BLOCK]
        q_b = queries[:, at].astype(BF16)
        v_b = r.v[at, :]
        marks = jnp.where(lower, tn(q_b, raised[:, at]), 0.0).astype(BF16)
        out_b = nn(marks, v_b)
        if b:
            out_b = out_b + tn(q_b, state.astype(BF16))
        r.head_local[at, :] = out_b
        r.q_lead[b] = (queries[:, at] * jnp.exp(lead)).astype(BF16)
        update = nn((keys[:, at] * jnp.exp(total - running[:, at])).astype(BF16), v_b)
        state = state * jnp.exp(total) + update
        lead = lead + total
    lead = jnp.broadcast_to(lead, (HEAD_K, 128)).T[:1]
    lead = jnp.concatenate([lead, jnp.zeros((1, 128 - HEAD_K), F32)], axis=1)
    r.own_state[...] = state.astype(BF16)
    r.own_log[...] = lead
    loaded(shared_loads)
    shared = nt(r.normed[...], r.sgu[...])
    shared = silu(shared[:, :64]) * shared[:, 64:]
    shared = jnp.concatenate([shared[: TOK_B // 2], shared[TOK_B // 2 :]], axis=1).astype(BF16)
    r.mixed[y, x, pl.ds(TOK_A, TOK_B // 2), :] = shared

    copies = []

    def send(source, target, device):
        n = len(copies)
        copy = pltpu.make_async_remote_copy(
            src_ref=source,
            dst_ref=target,
            send_sem=r.send_sem.at[n],
            recv_sem=r.recv_sem.at[n],
            device_id=device,
            device_id_type=MESH,
        )
        copies.append(copy)
        copy.start()
        return copy

    def main_rows(e):
        return pl.ds(pl.multiple_of(e * MAIN, MAIN), MAIN)

    def distance(k):
        return (k + 1) // 2 * (2 * lax.rem(k, 2) - 1)

    near = zs // 2
    section = r.section

    def pair_of_copies(main_from, main_to, left_from, left_to, sems, device):
        for n, source, target in ((0, main_from, main_to), (1, left_from, left_to)):
            send_sem, recv_sem = sems(n)
            if device is None:
                pltpu.make_async_copy(source, target, recv_sem).start()
            else:
                pltpu.make_async_remote_copy(
                    src_ref=source,
                    dst_ref=target,
                    send_sem=send_sem,
                    recv_sem=recv_sem,
                    device_id=device,
                    device_id_type=MESH,
                ).start()

    def give(e, k, device):
        chunk = 2 * (k // near) + c
        place = lax.rem(k, near)
        pair_of_copies(
            r.out_main.at[main_rows(e)],
            section.at[chunk, y, x, main_rows(place)],
            r.out_left.at[e],
            r.left_in.at[chunk, place],
            lambda n: (r.ep_send.at[0, n], r.ep_recv.at[n, chunk]),
            device,
        )

    def dispatch(i, carry):
        k = jnp.where(i < near, i, zs + near - 1 - i)
        to = lax.rem(z - distance(k) + zs, zs)
        for core in range(2):
            give(to * 2 + core, k, (to, core, y, x))
        return carry

    def give_back(chunk):
        first, core = near * (chunk // 2), chunk % 2

        def one(k, device):
            place = k - first
            to = lax.rem(z + distance(k) + zs, zs)
            pair_of_copies(
                r.back_main.at[chunk, main_rows(place)],
                r.returned.at[main_rows(me)],
                r.back_left.at[chunk, place],
                r.left_back.at[me],
                lambda n: (r.ep_send.at[1, n], r.back_recv.at[n]),
                device,
            )

        if first == 0:

            @pl.when(c == core)
            def _():
                one(jnp.int32(0), None)

            @pl.when(c != core)
            def _():
                one(jnp.int32(0), partner)

        start = 1 if first == 0 else 0

        def step_back(i, carry):
            k = first + near - 1 - i
            one(k, (lax.rem(z + distance(k) + zs, zs), core, y, x))
            return carry

        lax.fori_loop(0, near - start, step_back, 0)

    def arrived(main_ref, left_ref, main_sem, left_sem):
        pltpu.make_async_copy(main_ref, main_ref, main_sem).wait()
        pltpu.make_async_copy(left_ref, left_ref, left_sem).wait()

    def all_sent(sem):
        rest = r.out_main.at[pl.ds(0, (experts - 1) * MAIN)]
        pltpu.make_async_copy(rest, rest, r.ep_send.at[sem, 0]).wait()
        rest = r.out_left.at[pl.ds(0, experts - 1)]
        pltpu.make_async_copy(rest, rest, r.ep_send.at[sem, 1]).wait()

    pl.semaphore_wait(barrier, experts - 1 + 4)
    give(me, jnp.int32(0), None)
    give(z * 2 + 1 - c, jnp.int32(0), partner)
    lax.fori_loop(1, zs, dispatch, 0)
    to_state = send(r.own_state, r.mate_state, partner)
    to_log = send(r.own_log, r.mate_log, partner)

    wd_near = []
    for d, by_y, by_x in ((1, y_up, x_up), (-1, y_down, x_down)):
        wd_near.append(send(given.wd.at[turn(y, d)], r.wd1.at[y], by_y))
        wd_near.append(send(given.wd.at[:, turn(x, d)], r.wd2.at[x], by_x))
    lower_half, upper_half = pl.ds(0, RING // 2), pl.ds(RING // 2, RING // 2)

    def wd_walk():
        y_two, x_two = turn(y, 2), turn(x, 2)
        steps = [
            send(given.wd.at[y_two, lower_half], r.wd1_pass.at[0], y_up),
            send(given.wd.at[lower_half, x_two], r.wd2_pass.at[0], x_up),
            send(given.wd.at[y_two, upper_half], r.wd1_pass.at[1], y_down),
            send(given.wd.at[upper_half, x_two], r.wd2_pass.at[1], x_down),
        ]
        yield
        for copy in steps:
            copy.wait_recv()
        steps = [
            send(r.wd1_pass.at[0], r.wd1.at[turn(y, -1), lower_half], y_up),
            send(r.wd2_pass.at[0], r.wd2.at[turn(x, -1), lower_half], x_up),
            send(r.wd1_pass.at[1], r.wd1.at[turn(y, 1), upper_half], y_down),
            send(r.wd2_pass.at[1], r.wd2.at[turn(x, 1), upper_half], x_down),
        ]
        yield
        for copy in steps + wd_near:
            copy.wait_recv()

    to_state.wait_recv()
    to_log.wait_recv()
    mate = r.mate_state[...].astype(F32)
    mate_log = r.mate_log[...]
    first = jnp.where(c == 0, state, mate)
    second = jnp.where(c == 0, mate, state)
    second_log = jnp.where(c == 0, mate_log, lead)
    chip = as_column(jnp.exp(second_log))[:HEAD_K] * first + second
    low, high = chip[: HEAD_K // 2], chip[HEAD_K // 2 :]
    r.chip_state[...] = jnp.where(c == 0, low, high).astype(BF16)
    r.chip_log[...] = lead + mate_log

    def chip_copies(to):
        device = (to, c, y, x)
        return [
            pltpu.make_async_remote_copy(
                src_ref=source,
                dst_ref=target.at[z],
                send_sem=r.z_send.at[n, to],
                recv_sem=r.z_recv.at[n, z],
                device_id=device,
                device_id_type=MESH,
            )
            for n, source, target in (
                (0, r.chip_state, r.chip_in),
                (1, r.chip_log, r.chip_log_in),
            )
        ]

    def pass_on(to, carry):
        @pl.when(to > z)
        def _():
            for copy in chip_copies(to):
                copy.start()

        return carry

    lax.fori_loop(0, zs, pass_on, 0)

    def gather_part(buf, axis, start, middle, stop):
        whole, top, bottom = split_rows(start, stop), split_rows(start, middle), split_rows(middle, stop)
        if axis == "x":
            block = lambda d, rows: buf.at[y, turn(x, d), rows]
            slab = lambda d, rows: buf.at[turn(y, d), :, rows]
            up, down, then_up, then_down = x_up, x_down, y_up, y_down
        else:
            block = lambda d, rows: buf.at[turn(y, d), x, rows]
            slab = lambda d, rows: buf.at[:, turn(x, d), rows]
            up, down, then_up, then_down = y_up, y_down, x_up, x_down
        for piece, ahead, back in ((block, up, down), (slab, then_up, then_down)):
            a = send(piece(0, whole), piece(0, whole), ahead)
            b = send(piece(0, whole), piece(0, whole), back)
            yield
            a.wait_recv()
            a = send(piece(-1, top), piece(-1, top), ahead)
            b.wait_recv()
            b = send(piece(1, bottom), piece(1, bottom), back)
            yield
            a.wait_recv()
            b.wait_recv()

    def step(*walks):
        for walk in walks:
            next(walk, None)

    def mixer_walk():
        def take(to, carry):
            @pl.when(to < z)
            def _():
                for n, target in ((0, r.chip_in.at[to]), (1, r.chip_log_in.at[to])):
                    pltpu.make_async_copy(target, target, r.z_recv.at[n, to]).wait()

            return carry

        lax.fori_loop(0, zs, take, 0)
        after = jnp.zeros((1, 128), F32)
        factors = []
        for j in range(zs - 1, -1, -1):
            factors.append(jnp.where(j < z, jnp.exp(after), 0.0))
            after = after + jnp.where(j < z, r.chip_log_in[j], 0.0)
        factors = jnp.concatenate(factors[::-1] + [jnp.zeros((128 - zs, 128), F32)], axis=0).T
        factors = jnp.where(c == 0, factors[: HEAD_K // 2], factors[HEAD_K // 2 : HEAD_K])
        incoming = jnp.zeros((HEAD_K // 2, COLS), F32)
        for j in range(zs):
            incoming = incoming + factors[:, j : j + 1] * r.chip_in[j].astype(F32)
        r.incoming[c] = incoming.astype(BF16)
        to_incoming = send(r.incoming.at[c], r.incoming.at[c], partner)
        yield

        to_incoming.wait_recv()
        incoming = jnp.concatenate([r.incoming[0], r.incoming[1]], axis=0).astype(F32)
        incoming = jnp.where(
            c == 0, incoming, as_column(jnp.exp(mate_log))[:HEAD_K] * incoming + mate
        ).astype(BF16)
        heads = [tn(r.q_lead[b], incoming) for b in range(TOK_A // BLOCK)]
        heads = r.head_local[...] + jnp.concatenate(heads, axis=0)
        heads = heads * lax.rsqrt(jnp.mean(heads * heads, axis=1, keepdims=True) + EPS)
        heads = heads * r.hgain[...] * silu(r.og[...].astype(F32))
        r.mixed[y, x, pl.ds(0, TOK_A), :] = heads.astype(BF16)

    def flow(g):
        if g % 2 == 0:
            weight, mine, other = r.wd1, x, y
            ahead_dev, back_dev, then_ahead, then_back = x_up, x_down, y_up, y_down
        else:
            weight, mine, other = r.wd2, y, x
            ahead_dev, back_dev, then_ahead, then_back = y_up, y_down, x_up, x_down
        whole, top, bottom = pl.ds(0, CHUNK), pl.ds(0, TOP), pl.ds(TOP, CHUNK - TOP)
        rows = section.at[g]
        arrived(
            rows.at[y, x, pl.ds(0, CHUNK_MAIN)], r.left_in.at[g], r.ep_recv.at[0, g], r.ep_recv.at[1, g]
        )
        section[g, y, x, pl.ds(CHUNK_MAIN, CHUNK - CHUNK_MAIN), :] = jnp.concatenate(
            [r.left_in[g, e] for e in range(PER_CHUNK)], axis=0
        )
        yield from gather_part(rows, "xy"[g % 2], 0, TOP, CHUNK)
        lhs = jnp.concatenate(
            [section[g, a, b] for a in range(RING) for b in range(RING)], axis=1
        )
        hidden = r.hidden.at[g]
        hidden[mine] = (silu(nn(lhs, r.wg[...])) * nn(lhs, r.wu[...])).astype(BF16)
        piece = lambda d, part: hidden.at[turn(mine, d), part]
        a = send(piece(0, whole), piece(0, whole), ahead_dev)
        b = send(piece(0, whole), piece(0, whole), back_dev)
        yield
        a.wait_recv()
        a = send(piece(-1, top), piece(-1, top), ahead_dev)
        b.wait_recv()
        b = send(piece(1, bottom), piece(1, bottom), back_dev)
        yield
        a.wait_recv()
        b.wait_recv()

        def product(d):
            lhs = jnp.concatenate([hidden[i] for i in range(RING)], axis=1)
            return nn(lhs, weight[turn(other, d)].reshape(RING * 256, COLS))

        far, close = r.far.at[g], r.close.at[g]
        far[...] = product(2).astype(BF16)
        a = send(far.at[top], close.at[top], then_ahead)
        b = send(far.at[bottom], close.at[bottom], then_back)
        part = r.part.at[g]
        part[0] = product(1)
        part[1] = product(-1)
        part[2] = product(0)
        yield
        a.wait_recv()
        part[0, top] = part[0, top] + close[top].astype(F32)
        r.ahead[g] = part[0].astype(BF16)
        a = send(r.ahead.at[g], r.from_back.at[g], then_ahead)
        b.wait_recv()
        part[1, bottom] = part[1, bottom] + close[bottom].astype(F32)
        r.back[g] = part[1].astype(BF16)
        b = send(r.back.at[g], r.from_ahead.at[g], then_back)
        yield
        a.wait_recv()
        b.wait_recv()
        result = part[2] + r.from_back[g].astype(F32) + r.from_ahead[g].astype(F32)
        r.back_main[g] = result[:CHUNK_MAIN].astype(BF16)
        left = result[CHUNK_MAIN:].astype(BF16)
        for e in range(PER_CHUNK):
            r.back_left[g, e] = left[LEFT * e : LEFT * e + LEFT]
        give_back(g)

    def plane_walk():
        walk_a = gather_part(r.mixed, "x", 0, 80, 160)
        walk_b = gather_part(r.mixed, "y", 160, 224, MIX_ROWS)
        for _ in range(4):
            step(walk_a, walk_b)
            yield
        step(walk_a, walk_b)

    f0, f1, f2, f3 = [flow(g) for g in range(CHUNKS)]
    weights_in, mixing, mixed_out = wd_walk(), mixer_walk(), plane_walk()
    loaded(gate_loads)
    step(f0, f1)
    step(weights_in)
    step(f0, f1)
    step(f0, f1)
    step(f2, f3)
    step(weights_in)
    step(mixing)
    step(f0, f1)
    step(f2, f3)
    step(mixing)
    step(f0, f1)
    step(f2, f3)
    step(mixing)
    step(f0, f1)
    step(f2, f3)
    loaded(down_loads)
    step(weights_in)
    step(f0, f1)
    step(f2, f3)
    step(f0, f1)
    step(mixed_out)
    step(f2, f3)
    step(f0, f1)
    step(mixed_out)
    step(f2, f3)
    step(mixed_out)
    step(f2, f3)
    step(mixed_out)
    step(f2, f3)
    step(mixed_out)

    loaded(last_loads)
    mixed = r.mixed
    lhs = jnp.concatenate(
        [mixed[a, b, pl.ds(0, TOK_A), :] for a in range(RING) for b in range(RING)], axis=1
    )
    token_mixed[...] = nn(lhs, r.wo[...]).astype(BF16)
    lhs = jnp.concatenate(
        [mixed[a, b, pl.ds(TOK_A, TOK_B // 2), :] for a in range(RING) for b in range(RING)], axis=1
    )
    lane = lax.rem(lax.broadcasted_iota(jnp.int32, lhs.shape, 1), 128)
    zero = jnp.zeros_like(lhs)
    lhs = jnp.concatenate(
        [jnp.where(lane < 64, lhs, zero), jnp.where(lane < 64, zero, lhs)], axis=0
    )
    shared = nn(lhs, r.sd[...].reshape(2 * RING * RING * 64, COLS))

    returned = r.returned
    arrived(
        returned.at[pl.ds(0, MAIN_ROWS)], r.left_back, r.back_recv.at[0], r.back_recv.at[1]
    )
    returned[pl.ds(MAIN_ROWS, SLOTS - MAIN_ROWS), :] = jnp.concatenate(
        [r.left_back[e] for e in range(EXPERTS)], axis=0
    )
    total = shared + nn(r.mix_high[...], returned[...]) + nn(r.mix_low[...], returned[...])
    channel_mixed[...] = total.astype(BF16)

    for copy in copies:
        copy.wait_send()
    all_sent(0)
    all_sent(1)

    def passed(to, carry):
        @pl.when(to > z)
        def _():
            for copy in chip_copies(to):
                copy.wait_send()

        return carry

    lax.fori_loop(0, zs, passed, 0)


def solution(mesh):
    zs = mesh.shape["ep"] // 2
    torus = Mesh(mesh.devices.reshape(zs, 2, RING, RING), ("z", "c", "y", "x"))
    ep, tp = ("z", "c"), ("y", "x")

    def local(*args):
        given = Inputs(*args)
        given = given._replace(
            q=given.q.T,
            k=given.k.T,
            dec=given.dec.T,
            idx=given.idx.T,
            scores=given.scores.T,
            sg=given.sg.T,
            su=given.su.T,
            bias=given.bias.reshape(1, -1),
            hgain=given.hgain.reshape(1, -1),
            egain=given.egain.reshape(1, -1),
            wd=given.wd.reshape(RING, RING, 256, COLS),
            sd=given.sd.reshape(RING * RING, 64, COLS),
        )
        held = lambda shape, kind=BF16: pltpu.VMEM(shape, kind)
        like = lambda array: pltpu.VMEM(array.shape, array.dtype)
        dma = lambda *shape: pltpu.SemaphoreType.DMA(shape)
        scratch = dict(
            q=like(given.q),
            k=like(given.k),
            v=like(given.v),
            og=like(given.og),
            dec=like(given.dec),
            bias=like(given.bias),
            added=like(given.added),
            hgain=like(given.hgain),
            wo=like(given.wo),
            rows=like(given.rows),
            egain=like(given.egain),
            idx=like(given.idx),
            scores=like(given.scores),
            sgu=held((128, 2048)),
            wg=held((2048, 256)),
            wu=held((2048, 256)),
            wd1=held((RING, RING, 256, COLS)),
            wd2=held((RING, RING, 256, COLS)),
            sd=held((RING * RING, 2, 64, COLS)),
            normed=held((TOK_B, 2048)),
            out_main=held((MAIN_ROWS, COLS)),
            out_left=held((EXPERTS, LEFT, COLS)),
            left_in=held((CHUNKS, PER_CHUNK, LEFT, COLS)),
            section=held((CHUNKS, RING, RING, CHUNK, COLS)),
            mix_high=held((TOK_B, SLOTS)),
            mix_low=held((TOK_B, SLOTS)),
            head_local=held((TOK_A, COLS), F32),
            q_lead=held((TOK_A // BLOCK, HEAD_K, BLOCK)),
            own_state=held((HEAD_K, COLS)),
            mate_state=held((HEAD_K, COLS)),
            own_log=held((1, 128), F32),
            mate_log=held((1, 128), F32),
            chip_state=held((HEAD_K // 2, COLS)),
            chip_log=held((1, 128), F32),
            chip_in=held((zs, HEAD_K // 2, COLS)),
            chip_log_in=held((zs, 1, 128), F32),
            incoming=held((2, HEAD_K // 2, COLS)),
            mixed=held((RING, RING, MIX_ROWS, COLS)),
            hidden=held((CHUNKS, RING, CHUNK, 256)),
            far=held((CHUNKS, CHUNK, COLS)),
            close=held((CHUNKS, CHUNK, COLS)),
            ahead=held((CHUNKS, CHUNK, COLS)),
            back=held((CHUNKS, CHUNK, COLS)),
            from_ahead=held((CHUNKS, CHUNK, COLS)),
            from_back=held((CHUNKS, CHUNK, COLS)),
            part=held((CHUNKS, 3, CHUNK, COLS), F32),
            back_main=held((CHUNKS, CHUNK_MAIN, COLS)),
            back_left=held((CHUNKS, PER_CHUNK, LEFT, COLS)),
            wd1_pass=held((2, RING // 2, 256, COLS)),
            wd2_pass=held((2, RING // 2, 256, COLS)),
            returned=held((SLOTS, COLS)),
            left_back=held((EXPERTS, LEFT, COLS)),
            load_sem=dma(24),
            send_sem=dma(96),
            recv_sem=dma(96),
            ep_send=dma(2, 2),
            ep_recv=dma(2, CHUNKS),
            back_recv=dma(2),
            z_send=dma(2, zs),
            z_recv=dma(2, zs),
        )
        Scratch = namedtuple("Scratch", tuple(scratch))

        def kernel(*refs):
            n = len(given)
            layer_kernel(zs, Inputs(*refs[:n]), refs[n], refs[n + 1], Scratch(*refs[n + 2 :]))

        return pl.pallas_call(
            kernel,
            out_shape=(
                jax.ShapeDtypeStruct((TOK_A, COLS), BF16),
                jax.ShapeDtypeStruct((TOK_B, COLS), BF16),
            ),
            in_specs=[pl.BlockSpec(memory_space=pltpu.HBM)] * len(given),
            out_specs=(pl.BlockSpec(memory_space=pltpu.VMEM),) * 2,
            scratch_shapes=list(scratch.values()),
            compiler_params=pltpu.CompilerParams(
                collective_id=0, has_side_effects=True, vmem_limit_bytes=67043328
            ),
            name="layer",
        )(*given)

    return jax.shard_map(
        local,
        mesh=torus,
        in_specs=(
            P(ep, tp), P(ep, tp), P(ep, tp), P(ep, tp), P(ep, tp), P(tp), P(tp, ep), P(tp),
            P(None, tp), P(ep, None), P(), P(ep, None), P(ep, None), P(ep, None, tp),
            P(ep, None, tp), P(ep, None, tp), P(None, tp), P(None, tp), P(None, tp),
        ),
        out_specs=(P(ep, tp), P(ep, tp)),
        check_vma=False,
    )
```

time: 214 us -> 83.5 us (0.39)
  Pallas kernels: 0 us -> 80.6 us
  waiting for transfers between devices: 73.7 us -> 0 us
  blocking collectives: 71.6 us -> 0 us
  starting transfers between devices: 19.4 us -> 0 us
  between operations: 14.8 us -> 0.66 us
  matrix products: 12.1 us -> 0 us
  local copies, waits for them, and re-layouts: 13.8 us -> 2.09 us
  other arithmetic: 6.79 us -> 0 us
    pallas_call x0 -> x1, Pallas kernels: none -> 80.6 us  [local(): pl.pallas_call(kernel, out_shape=(jax.ShapeDtypeStruct((TOK_A, COLS), BF1...]
    all_to_all x3 -> x0, waiting for transfers between devices: 46.5 us -> none  [the longest x2 38.2 us: copy_for_each(): lax.all_to_all(jnp.broadcast_to(value[None], (size, *value.shape)), axis,...]
    all_to_all x3 -> x0, blocking collectives: 37 us -> none  [turned_blocks(): lax.all_to_all(parts, axes[k], split_axis=k, concat_axis=k, tiled=True)]
    all_gather x2 -> x0, blocking collectives: 34.7 us -> none  [collected_together(): both, at, found = (lax.all_gather(jnp.concatenate(lines), axis), 0, {})]
    all_gather x1 -> x0, waiting for transfers between devices: 27.2 us -> none  [sent_together(): lax.all_gather(both, axis, axis=dim, tiled=True)]
    all_to_all x3 -> x0, starting transfers between devices: 19.3 us -> none  [the longest x2 10.6 us: copy_for_each(): lax.all_to_all(jnp.broadcast_to(value[None], (size, *value.shape)), axis,...]
    dot_general x13 -> x0, matrix products: 12.1 us -> none  [the longest x1 4.06 us: local(): jnp.dot(routed_section, down_weight, preferred_element_type=jnp.float32)]
    gather x3 -> x0, local copies, waits for them, and re-layouts: 3.44 us -> none  [the longest x2 1.99 us: fill_slots(): picked_rows = jnp.take(source_rows, jnp.maximum(owners, 0), axis=0)]
  transfers between devices with their start and end apart: 4 -> 0, of which waited for: 4 -> 0; matrix products, arithmetic and copies ran while one was open for 5% -> 0% of each run, Pallas kernels for 0% -> 0%
where the time goes in v1:
time: 83.5 us; the launch traced here: 83.3 us
  Pallas kernels  80.6 us (97%)
  local copies, waits for them, and re-layouts  2.09 us (3%)
    pallas_call x1, Pallas kernels, local(): pl.pallas_call(kernel, out_shape=(jax.ShapeDtypeStruct((TOK_A, COLS), BF1...  80.6 us
    unnamed x4, local copies, waits for them, and re-layouts  2.09 us

profile of v1, /device:TPU:1, one launch (start us, length us, event | category | flops | bytes accessed | tf_op | source)
XLA Modules:
  0.0 83.3 jit_solution(5432770645009481609)
XLA Ops:
  0.6 80.6 %layer.1 = (bf16[256,128]{1,0:T(8,128)(2,1)}, bf16[96,128]{1,0:T(8,128)(2,1)}) custom-call(bf16[64,256]{1,0:T(8,128)(2,1)} %bitcast.16, bf16[64,256]{1,0:T(8,128)(2,1)} %bitcast.17, bf16[256,128]{1,0:T(8,128)(2,1)} %refs_2_.1, bf16[256,128]{1,0:T(8,128)(2,1)} %refs_3_.1, bf16[64,256]{1,0:T(8,128)(2,1)} %bitcast.18, f32[1,64]{1,0:T(1,128)} %bitcast.22, ...), custom_call_target="tpu_custom_call" | custom-call | tf_op jit(solution)/shard_map/layer/pallas_call | solution.py:720
  81.2 0.0 copy-start
  81.2 1.5 %copy.23 = bf16[256,128]{1,0:T(8,128)(2,1)} copy(bf16[256,128]{1,0:T(8,128)(2,1)} %get-tuple-element.4) | data formatting | bytes 131072
  82.7 0.0 copy-done
  82.7 0.6 copy.24
Async XLA Ops:
  81.2 1.5 %copy-start = (bf16[96,128]{1,0:T(8,128)(2,1)S(1)}, bf16[96,128]{1,0:T(8,128)(2,1)}, u32[]{:S(2)}) copy-start(bf16[96,128]{1,0:T(8,128)(2,1)} %get-tuple-element.5) | copy-start | bytes 73732

commit v2 on v1

--- a/solution.py
+++ b/solution.py
@@ -1,3 +1,4 @@
+import math
 from collections import namedtuple
 from typing import NamedTuple
 
@@ -13,6 +14,8 @@
 F32 = jnp.float32
 BF16 = jnp.bfloat16
 
+SENDS, RECEIVES = 14, 53
+DIRECT, MDIRECT = (2, 3), True
 EPS = 1e-06
 TEMPER = 16.0
 ROUTED_SCALE = 2.5
@@ -103,6 +106,8 @@
     x_up, x_down = (z, c, y, turn(x, 1)), (z, c, y, turn(x, -1))
     y_up, y_down = (z, c, turn(y, 1), x), (z, c, turn(y, -1), x)
 
+    x_far, y_far = (z, c, y, turn(x, 2)), (z, c, turn(y, 2), x)
+
     def ep_device(e):
         return (e // 2, lax.rem(e, 2), y, x)
 
@@ -118,6 +123,20 @@
         Load(given.rows, r.rows), Load(given.egain, r.egain),
         Load(given.idx, r.idx), Load(given.scores, r.scores),
     ]
+    r.chip_in[...] = jnp.zeros_like(r.chip_in)
+    r.chip_log_in[...] = jnp.zeros_like(r.chip_log_in)
+    barrier = pltpu.get_barrier_semaphore()
+
+    def greet(d, carry):
+        pl.semaphore_signal(
+            barrier, inc=1, device_id=ep_device(lax.rem(me + d, experts)), device_id_type=MESH
+        )
+        return carry
+
+    lax.fori_loop(1, experts, greet, 0)
+    for who in (x_up, x_down, y_up, y_down, x_far, y_far):
+        pl.semaphore_signal(barrier, inc=1, device_id=who, device_id_type=MESH)
+
     mixer_loads = [
         Load(given.dec, r.dec), Load(given.bias, r.bias), Load(given.added, r.added),
         Load(given.k, r.k), Load(given.v, r.v), Load(given.q, r.q),
@@ -133,20 +152,6 @@
     def loaded(group):
         for item in group:
             item.copy.wait()
-
-    r.chip_in[...] = jnp.zeros_like(r.chip_in)
-    r.chip_log_in[...] = jnp.zeros_like(r.chip_log_in)
-    barrier = pltpu.get_barrier_semaphore()
-
-    def greet(d, carry):
-        pl.semaphore_signal(
-            barrier, inc=1, device_id=ep_device(lax.rem(me + d, experts)), device_id_type=MESH
-        )
-        return carry
-
-    lax.fori_loop(1, experts, greet, 0)
-    for who in (x_up, x_down, y_up, y_down):
-        pl.semaphore_signal(barrier, inc=1, device_id=who, device_id_type=MESH)
 
     loaded(rows_loads)
     features = r.rows[...].astype(F32)
@@ -191,14 +196,155 @@
 
     store_left(r.out_left, slots[MAIN_ROWS:])
 
-    owner, place = slot_parts(lax.broadcasted_iota(jnp.int32, (EXPERTS, SLOTS), 1))
-    spread = owner == lax.broadcasted_iota(jnp.int32, (EXPERTS, SLOTS), 0)
-    spread = jnp.where(spread, 1.0, 0.0).astype(BF16)
-    here = tn(rank, spread) == place[:1].astype(F32)
-    share_high = share.astype(BF16)
-    share_low = (share - share_high.astype(F32)).astype(BF16)
-    r.mix_high[...] = jnp.where(here, tn(share_high, spread), 0.0).astype(BF16)
-    r.mix_low[...] = jnp.where(here, tn(share_low, spread), 0.0).astype(BF16)
+    sent_rows = [0]
+    receivers = []
+
+    def receiver():
+        receivers.append(len(receivers))
+        return receivers[-1]
+
+    def send(source, target, device, recv):
+        rows = math.prod(source.shape) * source.dtype.itemsize // (2 * COLS)
+        if sent_rows[-1] + rows > r.wo.shape[0]:
+            sent_rows.append(0)
+        sent_rows[-1] += rows
+        pltpu.make_async_remote_copy(
+            src_ref=source,
+            dst_ref=target,
+            send_sem=r.send_sem.at[len(sent_rows) - 1],
+            recv_sem=r.recv_sem.at[recv],
+            device_id=device,
+            device_id_type=MESH,
+        ).start()
+
+    def landed(ref, recv):
+        pltpu.make_async_copy(ref, ref, r.recv_sem.at[recv]).wait()
+
+    def main_rows(e):
+        return pl.ds(pl.multiple_of(e * MAIN, MAIN), MAIN)
+
+    def distance(k):
+        return (k + 1) // 2 * (2 * lax.rem(k, 2) - 1)
+
+    near = zs // 2
+    section = r.section
+
+    def pair_of_copies(main_from, main_to, left_from, left_to, sems, device):
+        for n, source, target in ((0, main_from, main_to), (1, left_from, left_to)):
+            send_sem, recv_sem = sems(n)
+            if device is None:
+                pltpu.make_async_copy(source, target, recv_sem).start()
+            else:
+                pltpu.make_async_remote_copy(
+                    src_ref=source,
+                    dst_ref=target,
+                    send_sem=send_sem,
+                    recv_sem=recv_sem,
+                    device_id=device,
+                    device_id_type=MESH,
+                ).start()
+
+    def give(e, k, device):
+        chunk = 2 * (k // near) + c
+        place = lax.rem(k, near)
+        pair_of_copies(
+            r.out_main.at[main_rows(e)],
+            section.at[chunk, y, x, main_rows(place)],
+            r.out_left.at[e],
+            r.left_in.at[chunk, place],
+            lambda n: (r.ep_send.at[0, n], r.ep_recv.at[n, chunk]),
+            device,
+        )
+
+    def dispatch(i, carry):
+        k = jnp.where(i < near, i, zs + near - 1 - i)
+        to = lax.rem(z - distance(k) + zs, zs)
+        for core in range(2):
+            give(to * 2 + core, k, (to, core, y, x))
+        return carry
+
+    def give_back(chunk):
+        first, core = near * (chunk // 2), chunk % 2
+
+        def one(k, device):
+            place = k - first
+            to = lax.rem(z + distance(k) + zs, zs)
+            pair_of_copies(
+                r.back_main.at[chunk, main_rows(place)],
+                r.returned.at[main_rows(me)],
+                r.back_left.at[chunk, place],
+                r.left_back.at[me],
+                lambda n: (r.ep_send.at[1, n], r.back_recv.at[n]),
+                device,
+            )
+
+        if first == 0:
+
+            @pl.when(c == core)
+            def _():
+                one(jnp.int32(0), None)
+
+            @pl.when(c != core)
+            def _():
+                one(jnp.int32(0), partner)
+
+        start = 1 if first == 0 else 0
+
+        def step_back(i, carry):
+            k = first + near - 1 - i
+            one(k, (lax.rem(z + distance(k) + zs, zs), core, y, x))
+            return carry
+
+        lax.fori_loop(0, near - start, step_back, 0)
+
+    def arrived(main_ref, left_ref, main_sem, left_sem):
+        pltpu.make_async_copy(main_ref, main_ref, main_sem).wait()
+        pltpu.make_async_copy(left_ref, left_ref, left_sem).wait()
+
+    def all_sent(sem):
+        rest = r.out_main.at[pl.ds(0, (experts - 1) * MAIN)]
+        pltpu.make_async_copy(rest, rest, r.ep_send.at[sem, 0]).wait()
+        rest = r.out_left.at[pl.ds(0, experts - 1)]
+        pltpu.make_async_copy(rest, rest, r.ep_send.at[sem, 1]).wait()
+
+    pl.semaphore_wait(barrier, experts - 1 + 6)
+    give(me, jnp.int32(0), None)
+    give(z * 2 + 1 - c, jnp.int32(0), partner)
+    lax.fori_loop(1, zs, dispatch, 0)
+    def wd_walk():
+        y_two, x_two = turn(y, 2), turn(x, 2)
+        pass_in = [(receiver(), receiver()) for _ in range(2)]
+        wd1_in, wd2_in = receiver(), receiver()
+        for j, (by_y, by_x) in enumerate(pass_in):
+            for at, y_side, x_side in ((j, y_up, x_up), (j + 2, y_down, x_down)):
+                send(given.wd.at[y_two, at], r.wd1_pass.at[at], y_side, by_y)
+                send(given.wd.at[at, x_two], r.wd2_pass.at[at], x_side, by_x)
+            yield
+        for j in range(RING):
+            for d, y_side, x_side in ((1, y_up, x_up), (-1, y_down, x_down)):
+                send(given.wd.at[turn(y, d), j], r.wd1.at[y, j], y_side, wd1_in)
+                send(given.wd.at[j, turn(x, d)], r.wd2.at[x, j], x_side, wd2_in)
+            yield
+        for j, (by_y, by_x) in enumerate(pass_in):
+            landed(r.wd1_pass.at[pl.ds(0, 2)], by_y)
+            landed(r.wd2_pass.at[pl.ds(0, 2)], by_x)
+            for at, d, y_side, x_side in ((j, -1, y_up, x_up), (j + 2, 1, y_down, x_down)):
+                send(r.wd1_pass.at[at], r.wd1.at[turn(y, d), at], y_side, wd1_in)
+                send(r.wd2_pass.at[at], r.wd2.at[turn(x, d), at], x_side, wd2_in)
+            yield
+        landed(r.wd1.at[pl.ds(0, 3)], wd1_in)
+        landed(r.wd2.at[pl.ds(0, 3)], wd2_in)
+
+    def step(*walks):
+        for walk in walks:
+            next(walk, None)
+
+    weights_in = wd_walk()
+    step(weights_in)
+    step(weights_in)
+    step(weights_in)
+    step(weights_in)
+    step(weights_in)
 
     loaded(mixer_loads)
     logits = r.dec[...].astype(F32) + as_column(r.bias[...])[:, :1]
@@ -233,154 +379,30 @@
     lead = jnp.broadcast_to(lead, (HEAD_K, 128)).T[:1]
     lead = jnp.concatenate([lead, jnp.zeros((1, 128 - HEAD_K), F32)], axis=1)
     r.own_state[...] = state.astype(BF16)
-    r.own_log[...] = lead
+    r.own_log[...] = jnp.broadcast_to(lead, (8, 128))
+    state_in, log_in, incoming_in = receiver(), receiver(), receiver()
+    send(r.own_state, r.mate_state, partner, state_in)
+    send(r.own_log, r.mate_log, partner, log_in)
+
+    owner, place = slot_parts(lax.broadcasted_iota(jnp.int32, (EXPERTS, SLOTS), 1))
+    spread = owner == lax.broadcasted_iota(jnp.int32, (EXPERTS, SLOTS), 0)
+    spread = jnp.where(spread, 1.0, 0.0).astype(BF16)
+    here = tn(rank, spread) == place[:1].astype(F32)
+    share_high = share.astype(BF16)
+    share_low = (share - share_high.astype(F32)).astype(BF16)
+    r.mix_high[...] = jnp.where(here, tn(share_high, spread), 0.0).astype(BF16)
+    r.mix_low[...] = jnp.where(here, tn(share_low, spread), 0.0).astype(BF16)
+
     loaded(shared_loads)
     shared = nt(r.normed[...], r.sgu[...])
     shared = silu(shared[:, :64]) * shared[:, 64:]
     shared = jnp.concatenate([shared[: TOK_B // 2], shared[TOK_B // 2 :]], axis=1).astype(BF16)
     r.mixed[y, x, pl.ds(TOK_A, TOK_B // 2), :] = shared
 
-    copies = []
-
-    def send(source, target, device):
-        n = len(copies)
-        copy = pltpu.make_async_remote_copy(
-            src_ref=source,
-            dst_ref=target,
-            send_sem=r.send_sem.at[n],
-            recv_sem=r.recv_sem.at[n],
-            device_id=device,
-            device_id_type=MESH,
-        )
-        copies.append(copy)
-        copy.start()
-        return copy
-
-    def main_rows(e):
-        return pl.ds(pl.multiple_of(e * MAIN, MAIN), MAIN)
-
-    def distance(k):
-        return (k + 1) // 2 * (2 * lax.rem(k, 2) - 1)
-
-    near = zs // 2
-    section = r.section
-
-    def pair_of_copies(main_from, main_to, left_from, left_to, sems, device):
-        for n, source, target in ((0, main_from, main_to), (1, left_from, left_to)):
-            send_sem, recv_sem = sems(n)
-            if device is None:
-                pltpu.make_async_copy(source, target, recv_sem).start()
-            else:
-                pltpu.make_async_remote_copy(
-                    src_ref=source,
-                    dst_ref=target,
-                    send_sem=send_sem,
-                    recv_sem=recv_sem,
-                    device_id=device,
-                    device_id_type=MESH,
-                ).start()
-
-    def give(e, k, device):
-        chunk = 2 * (k // near) + c
-        place = lax.rem(k, near)
-        pair_of_copies(
-            r.out_main.at[main_rows(e)],
-            section.at[chunk, y, x, main_rows(place)],
-            r.out_left.at[e],
-            r.left_in.at[chunk, place],
-            lambda n: (r.ep_send.at[0, n], r.ep_recv.at[n, chunk]),
-            device,
-        )
-
-    def dispatch(i, carry):
-        k = jnp.where(i < near, i, zs + near - 1 - i)
-        to = lax.rem(z - distance(k) + zs, zs)
-        for core in range(2):
-            give(to * 2 + core, k, (to, core, y, x))
-        return carry
-
-    def give_back(chunk):
-        first, core = near * (chunk // 2), chunk % 2
-
-        def one(k, device):
-            place = k - first
-            to = lax.rem(z + distance(k) + zs, zs)
-            pair_of_copies(
-                r.back_main.at[chunk, main_rows(place)],
-                r.returned.at[main_rows(me)],
-                r.back_left.at[chunk, place],
-                r.left_back.at[me],
-                lambda n: (r.ep_send.at[1, n], r.back_recv.at[n]),
-                device,
-            )
-
-        if first == 0:
-
-            @pl.when(c == core)
-            def _():
-                one(jnp.int32(0), None)
-
-            @pl.when(c != core)
-            def _():
-                one(jnp.int32(0), partner)
-
-        start = 1 if first == 0 else 0
-
-        def step_back(i, carry):
-            k = first + near - 1 - i
-            one(k, (lax.rem(z + distance(k) + zs, zs), core, y, x))
-            return carry
-
-        lax.fori_loop(0, near - start, step_back, 0)
-
-    def arrived(main_ref, left_ref, main_sem, left_sem):
-        pltpu.make_async_copy(main_ref, main_ref, main_sem).wait()
-        pltpu.make_async_copy(left_ref, left_ref, left_sem).wait()
-
-    def all_sent(sem):
-        rest = r.out_main.at[pl.ds(0, (experts - 1) * MAIN)]
-        pltpu.make_async_copy(rest, rest, r.ep_send.at[sem, 0]).wait()
-        rest = r.out_left.at[pl.ds(0, experts - 1)]
-        pltpu.make_async_copy(rest, rest, r.ep_send.at[sem, 1]).wait()
-
-    pl.semaphore_wait(barrier, experts - 1 + 4)
-    give(me, jnp.int32(0), None)
-    give(z * 2 + 1 - c, jnp.int32(0), partner)
-    lax.fori_loop(1, zs, dispatch, 0)
-    to_state = send(r.own_state, r.mate_state, partner)
-    to_log = send(r.own_log, r.mate_log, partner)
-
-    wd_near = []
-    for d, by_y, by_x in ((1, y_up, x_up), (-1, y_down, x_down)):
-        wd_near.append(send(given.wd.at[turn(y, d)], r.wd1.at[y], by_y))
-        wd_near.append(send(given.wd.at[:, turn(x, d)], r.wd2.at[x], by_x))
-    lower_half, upper_half = pl.ds(0, RING // 2), pl.ds(RING // 2, RING // 2)
-
-    def wd_walk():
-        y_two, x_two = turn(y, 2), turn(x, 2)
-        steps = [
-            send(given.wd.at[y_two, lower_half], r.wd1_pass.at[0], y_up),
-            send(given.wd.at[lower_half, x_two], r.wd2_pass.at[0], x_up),
-            send(given.wd.at[y_two, upper_half], r.wd1_pass.at[1], y_down),
-            send(given.wd.at[upper_half, x_two], r.wd2_pass.at[1], x_down),
-        ]
-        yield
-        for copy in steps:
-            copy.wait_recv()
-        steps = [
-            send(r.wd1_pass.at[0], r.wd1.at[turn(y, -1), lower_half], y_up),
-            send(r.wd2_pass.at[0], r.wd2.at[turn(x, -1), lower_half], x_up),
-            send(r.wd1_pass.at[1], r.wd1.at[turn(y, 1), upper_half], y_down),
-            send(r.wd2_pass.at[1], r.wd2.at[turn(x, 1), upper_half], x_down),
-        ]
-        yield
-        for copy in steps + wd_near:
-            copy.wait_recv()
-
-    to_state.wait_recv()
-    to_log.wait_recv()
+    landed(r.mate_state, state_in)
+    landed(r.mate_log, log_in)
     mate = r.mate_state[...].astype(F32)
-    mate_log = r.mate_log[...]
+    mate_log = r.mate_log[:1]
     first = jnp.where(c == 0, state, mate)
     second = jnp.where(c == 0, mate, state)
     second_log = jnp.where(c == 0, mate_log, lead)
@@ -416,31 +438,51 @@
 
     lax.fori_loop(0, zs, pass_on, 0)
 
-    def gather_part(buf, axis, start, middle, stop):
+    def gather_part(buf, axis, start, middle, stop, direct):
         whole, top, bottom = split_rows(start, stop), split_rows(start, middle), split_rows(middle, stop)
         if axis == "x":
             block = lambda d, rows: buf.at[y, turn(x, d), rows]
             slab = lambda d, rows: buf.at[turn(y, d), :, rows]
-            up, down, then_up, then_down = x_up, x_down, y_up, y_down
+            up, down, far, then_up, then_down = x_up, x_down, x_far, y_up, y_down
         else:
             block = lambda d, rows: buf.at[turn(y, d), x, rows]
             slab = lambda d, rows: buf.at[:, turn(x, d), rows]
-            up, down, then_up, then_down = y_up, y_down, x_up, x_down
-        for piece, ahead, back in ((block, up, down), (slab, then_up, then_down)):
-            a = send(piece(0, whole), piece(0, whole), ahead)
-            b = send(piece(0, whole), piece(0, whole), back)
+            up, down, far, then_up, then_down = y_up, y_down, y_far, x_up, x_down
+        from_down, from_up, from_far = receiver(), receiver(), receiver()
+        then_from_down, then_from_up, then_from_far = receiver(), receiver(), receiver()
+
+        def out(piece, device, recv):
+            send(piece, piece, device, recv)
+
+        def over(d):
+            out(block(d, whole), then_up, then_from_down)
+            out(block(d, whole), then_down, then_from_up)
+
+        out(block(0, whole), up, from_down)
+        out(block(0, whole), down, from_up)
+        if direct:
+            out(block(0, whole), far, from_far)
+        over(0)
+        yield
+        landed(block(-1, whole), from_down)
+        if not direct:
+            out(block(-1, top), up, from_far)
+        over(-1)
+        landed(block(1, whole), from_up)
+        if not direct:
+            out(block(1, bottom), down, from_far)
+        over(1)
+        if not direct:
             yield
-            a.wait_recv()
-            a = send(piece(-1, top), piece(-1, top), ahead)
-            b.wait_recv()
-            b = send(piece(1, bottom), piece(1, bottom), back)
-            yield
-            a.wait_recv()
-            b.wait_recv()
-
-    def step(*walks):
-        for walk in walks:
-            next(walk, None)
+        landed(block(2, whole), from_far)
+        over(2)
+        yield
+        landed(slab(-1, whole), then_from_down)
+        out(slab(-1, top), then_up, then_from_far)
+        landed(slab(1, whole), then_from_up)
+        out(slab(1, bottom), then_down, then_from_far)
+        yield
+        landed(slab(2, whole), then_from_far)
 
     def mixer_walk():
         def take(to, carry):
@@ -463,10 +505,10 @@
         for j in range(zs):
             incoming = incoming + factors[:, j : j + 1] * r.chip_in[j].astype(F32)
         r.incoming[c] = incoming.astype(BF16)
-        to_incoming = send(r.incoming.at[c], r.incoming.at[c], partner)
+        send(r.incoming.at[c], r.incoming.at[c], partner, incoming_in)
         yield
 
-        to_incoming.wait_recv()
+        landed(r.incoming.at[1 - c], incoming_in)
         incoming = jnp.concatenate([r.incoming[0], r.incoming[1]], axis=0).astype(F32)
         incoming = jnp.where(
             c == 0, incoming, as_column(jnp.exp(mate_log))[:HEAD_K] * incoming + mate
@@ -481,10 +523,11 @@
         if g % 2 == 0:
             weight, mine, other = r.wd1, x, y
             ahead_dev, back_dev, then_ahead, then_back = x_up, x_down, y_up, y_down
+            far_dev, then_far = x_far, y_far
         else:
             weight, mine, other = r.wd2, y, x
             ahead_dev, back_dev, then_ahead, then_back = y_up, y_down, x_up, x_down
-        whole, top, bottom = pl.ds(0, CHUNK), pl.ds(0, TOP), pl.ds(TOP, CHUNK - TOP)
+            far_dev, then_far = y_far, x_far
         rows = section.at[g]
         arrived(
             rows.at[y, x, pl.ds(0, CHUNK_MAIN)], r.left_in.at[g], r.ep_recv.at[0, g], r.ep_recv.at[1, g]
@@ -492,49 +535,31 @@
         section[g, y, x, pl.ds(CHUNK_MAIN, CHUNK - CHUNK_MAIN), :] = jnp.concatenate(
             [r.left_in[g, e] for e in range(PER_CHUNK)], axis=0
         )
-        yield from gather_part(rows, "xy"[g % 2], 0, TOP, CHUNK)
+        yield from gather_part(rows, "xy"[g % 2], 0, TOP, CHUNK, g in DIRECT)
         lhs = jnp.concatenate(
             [section[g, a, b] for a in range(RING) for b in range(RING)], axis=1
         )
         hidden = r.hidden.at[g]
         hidden[mine] = (silu(nn(lhs, r.wg[...])) * nn(lhs, r.wu[...])).astype(BF16)
-        piece = lambda d, part: hidden.at[turn(mine, d), part]
-        a = send(piece(0, whole), piece(0, whole), ahead_dev)
-        b = send(piece(0, whole), piece(0, whole), back_dev)
+        hidden_in, parts_in = receiver(), receiver()
+        for device in (far_dev, ahead_dev, back_dev):
+            send(hidden.at[mine], hidden.at[mine], device, hidden_in)
         yield
-        a.wait_recv()
-        a = send(piece(-1, top), piece(-1, top), ahead_dev)
-        b.wait_recv()
-        b = send(piece(1, bottom), piece(1, bottom), back_dev)
-        yield
-        a.wait_recv()
-        b.wait_recv()
+        landed(hidden.at[pl.ds(0, 3)], hidden_in)
 
         def product(d):
             lhs = jnp.concatenate([hidden[i] for i in range(RING)], axis=1)
             return nn(lhs, weight[turn(other, d)].reshape(RING * 256, COLS))
 
-        far, close = r.far.at[g], r.close.at[g]
-        far[...] = product(2).astype(BF16)
-        a = send(far.at[top], close.at[top], then_ahead)
-        b = send(far.at[bottom], close.at[bottom], then_back)
-        part = r.part.at[g]
-        part[0] = product(1)
-        part[1] = product(-1)
-        part[2] = product(0)
+        for n, d, device in ((0, 2, then_far), (1, 1, then_ahead), (2, -1, then_back)):
+            r.part[g, n] = product(d).astype(BF16)
+            send(r.part.at[g, n], r.parts_in.at[g, n], device, parts_in)
+        r.own_part[g] = product(0)
         yield
-        a.wait_recv()
-        part[0, top] = part[0, top] + close[top].astype(F32)
-        r.ahead[g] = part[0].astype(BF16)
-        a = send(r.ahead.at[g], r.from_back.at[g], then_ahead)
-        b.wait_recv()
-        part[1, bottom] = part[1, bottom] + close[bottom].astype(F32)
-        r.back[g] = part[1].astype(BF16)
-        b = send(r.back.at[g], r.from_ahead.at[g], then_back)
-        yield
-        a.wait_recv()
-        b.wait_recv()
-        result = part[2] + r.from_back[g].astype(F32) + r.from_ahead[g].astype(F32)
+        landed(r.parts_in.at[g], parts_in)
+        result = r.own_part[g]
+        for n in range(3):
+            result = result + r.parts_in[g, n].astype(F32)
         r.back_main[g] = result[:CHUNK_MAIN].astype(BF16)
         left = result[CHUNK_MAIN:].astype(BF16)
         for e in range(PER_CHUNK):
@@ -542,46 +567,22 @@
         give_back(g)
 
     def plane_walk():
-        walk_a = gather_part(r.mixed, "x", 0, 80, 160)
-        walk_b = gather_part(r.mixed, "y", 160, 224, MIX_ROWS)
-        for _ in range(4):
+        walk_a = gather_part(r.mixed, "x", 0, 80, 160, MDIRECT)
+        walk_b = gather_part(r.mixed, "y", 160, 224, MIX_ROWS, MDIRECT)
+        for _ in range(3 if MDIRECT else 4):
             step(walk_a, walk_b)
             yield
         step(walk_a, walk_b)
 
     f0, f1, f2, f3 = [flow(g) for g in range(CHUNKS)]
-    weights_in, mixing, mixed_out = wd_walk(), mixer_walk(), plane_walk()
-    loaded(gate_loads)
-    step(f0, f1)
-    step(weights_in)
-    step(f0, f1)
-    step(f0, f1)
-    step(f2, f3)
-    step(weights_in)
-    step(mixing)
-    step(f0, f1)
-    step(f2, f3)
-    step(mixing)
-    step(f0, f1)
-    step(f2, f3)
-    step(mixing)
-    step(f0, f1)
-    step(f2, f3)
-    loaded(down_loads)
-    step(weights_in)
-    step(f0, f1)
-    step(f2, f3)
-    step(f0, f1)
-    step(mixed_out)
-    step(f2, f3)
-    step(f0, f1)
-    step(mixed_out)
-    step(f2, f3)
-    step(mixed_out)
-    step(f2, f3)
-    step(mixed_out)
-    step(f2, f3)
-    step(mixed_out)
+    mixing, mixed_out = mixer_walk(), plane_walk()
+    loaded(gate_loads + down_loads)
+    near_chunks, far_chunks = (f0, f1), (f2, f3)
+    A, B, W, X, M = near_chunks, far_chunks, (weights_in,), (mixing,), (mixed_out,)
+    for walks in (
+        A, W, A, B, W, A, X, B, W, A, X, B, W, A, X, B, M, A, B, M, A, B, M, M,
+    ):
+        step(*walks)
 
     loaded(last_loads)
     mixed = r.mixed
@@ -609,8 +610,9 @@
     total = shared + nn(r.mix_high[...], returned[...]) + nn(r.mix_low[...], returned[...])
     channel_mixed[...] = total.astype(BF16)
 
-    for copy in copies:
-        copy.wait_send()
+    for n, rows in enumerate(sent_rows):
+        rows = r.wo.at[pl.ds(0, rows)]
+        pltpu.make_async_copy(rows, rows, r.send_sem.at[n]).wait()
     all_sent(0)
     all_sent(1)
 
@@ -680,8 +682,8 @@
             q_lead=held((TOK_A // BLOCK, HEAD_K, BLOCK)),
             own_state=held((HEAD_K, COLS)),
             mate_state=held((HEAD_K, COLS)),
-            own_log=held((1, 128), F32),
-            mate_log=held((1, 128), F32),
+            own_log=held((8, 128), F32),
+            mate_log=held((8, 128), F32),
             chip_state=held((HEAD_K // 2, COLS)),
             chip_log=held((1, 128), F32),
             chip_in=held((zs, HEAD_K // 2, COLS)),
@@ -689,22 +691,18 @@
             incoming=held((2, HEAD_K // 2, COLS)),
             mixed=held((RING, RING, MIX_ROWS, COLS)),
             hidden=held((CHUNKS, RING, CHUNK, 256)),
-            far=held((CHUNKS, CHUNK, COLS)),
-            close=held((CHUNKS, CHUNK, COLS)),
-            ahead=held((CHUNKS, CHUNK, COLS)),
-            back=held((CHUNKS, CHUNK, COLS)),
-            from_ahead=held((CHUNKS, CHUNK, COLS)),
-            from_back=held((CHUNKS, CHUNK, COLS)),
-            part=held((CHUNKS, 3, CHUNK, COLS), F32),
+            part=held((CHUNKS, 3, CHUNK, COLS)),
+            parts_in=held((CHUNKS, 3, CHUNK, COLS)),
+            own_part=held((CHUNKS, CHUNK, COLS), F32),
             back_main=held((CHUNKS, CHUNK_MAIN, COLS)),
             back_left=held((CHUNKS, PER_CHUNK, LEFT, COLS)),
-            wd1_pass=held((2, RING // 2, 256, COLS)),
-            wd2_pass=held((2, RING // 2, 256, COLS)),
+            wd1_pass=held((RING, 256, COLS)),
+            wd2_pass=held((RING, 256, COLS)),
             returned=held((SLOTS, COLS)),
             left_back=held((EXPERTS, LEFT, COLS)),
-            load_sem=dma(24),
-            send_sem=dma(96),
-            recv_sem=dma(96),
+            load_sem=dma(21),
+            send_sem=dma(SENDS),
+            recv_sem=dma(RECEIVES),
             ep_send=dma(2, 2),
             ep_recv=dma(2, CHUNKS),
             back_recv=dma(2),

time: 83.5 us -> 72.1 us (0.86)
  Pallas kernels: 80.6 us -> 69.2 us
    pallas_call x1, Pallas kernels: 80.6 us -> 69.2 us  [local(): pl.pallas_call(kernel, out_shape=(jax.ShapeDtypeStruct((TOK_A, COLS), BF1...]
where the time goes in v2:
time: 72.1 us; the launch traced here: 72 us
  Pallas kernels  69.2 us (96%)
  local copies, waits for them, and re-layouts  2.09 us (3%)
    pallas_call x1, Pallas kernels, local(): pl.pallas_call(kernel, out_shape=(jax.ShapeDtypeStruct((TOK_A, COLS), BF1...  69.2 us
    unnamed x4, local copies, waits for them, and re-layouts  2.09 us

profile of v2, /device:TPU:1, one launch (start us, length us, event | category | flops | bytes accessed | tf_op | source)
XLA Modules:
  0.0 72.0 jit_solution(10285248015525068557)
XLA Ops:
  0.6 69.2 %layer.1 = (bf16[256,128]{1,0:T(8,128)(2,1)}, bf16[96,128]{1,0:T(8,128)(2,1)}) custom-call(bf16[64,256]{1,0:T(8,128)(2,1)} %bitcast.16, bf16[64,256]{1,0:T(8,128)(2,1)} %bitcast.17, bf16[256,128]{1,0:T(8,128)(2,1)} %refs_2_.1, bf16[256,128]{1,0:T(8,128)(2,1)} %refs_3_.1, bf16[64,256]{1,0:T(8,128)(2,1)} %bitcast.18, f32[1,64]{1,0:T(1,128)} %bitcast.22, ...), custom_call_target="tpu_custom_call" | custom-call | tf_op jit(solution)/shard_map/layer/pallas_call | solution.py:718
  69.9 0.0 copy-start
  69.9 1.5 %copy.23 = bf16[256,128]{1,0:T(8,128)(2,1)} copy(bf16[256,128]{1,0:T(8,128)(2,1)} %get-tuple-element.4) | data formatting | bytes 131072
  71.3 0.0 copy-done
  71.3 0.6 copy.24
Async XLA Ops:
  69.9 1.5 %copy-start = (bf16[96,128]{1,0:T(8,128)(2,1)S(1)}, bf16[96,128]{1,0:T(8,128)(2,1)}, u32[]{:S(2)}) copy-start(bf16[96,128]{1,0:T(8,128)(2,1)} %get-tuple-element.5) | copy-start | bytes 73732
